TPU v7x, 128 devices: a whole 4x4x4 slice. The times are simulated.
128 devices in a mesh: ep: 64 (over z, y, x), tp: 2 (over core).
Axes of the slice: x: 4, y: 4, z: 4, core: 2. Of those that a mesh axis runs over, the one named last changes fastest.
Arguments:
- tokens: bfloat16 [4096, 2048], P('ep', 'tp'), may hold values from -6 to 6
- sequence_state_real: float32 [4096, 128, 64], P('ep', 'tp'), may hold values from -4 to 4
- sequence_state_imaginary: float32 [4096, 128, 64], P('ep', 'tp'), may hold values from -4 to 4
- mixer_norm_gain: float32 [2048], replicated, may hold values from 0.1 to 1.9
- expert_norm_gain: float32 [2048], replicated, may hold values from 0.1 to 1.9
- rate: float32 [128, 64], P('tp'), may hold values from 0.1 to 4
- freq: float32 [128, 64], P('tp'), may hold values from -3 to 3
- log_group_step: float32 [128], P('tp'), may hold values from -3 to 0
- input_map_real: float32 [128, 64, 16], P('tp'), may hold values from -1 to 1
- input_map_imaginary: float32 [128, 64, 16], P('tp'), may hold values from -1 to 1
- output_map_real: float32 [128, 16, 64], P('tp'), may hold values from -0.75 to 0.75
- output_map_imaginary: float32 [128, 16, 64], P('tp'), may hold values from -0.75 to 0.75
- skip: float32 [2048], P('tp'), may hold values from -4 to 4
- mixer_value_weight: bfloat16 [2048, 2048], P('tp'), may hold values from -0.125 to 0.125
- mixer_gate_weight: bfloat16 [2048, 2048], P('tp'), may hold values from -0.125 to 0.125
- group_router_weight: bfloat16 [2048, 4], replicated, may hold values from -0.125 to 0.125
- expert_router_weight: bfloat16 [2048, 64], replicated, may hold values from -0.125 to 0.125
- dense_blend_weight: float32 [2048], replicated, may hold values from -0.125 to 0.125
- routes: int32 [4096, 2], P('ep'), may hold values from 0 to 63, all different within a row; in each aligned block of 64 rows (0 to 63, 64 to 127, ...) at most 4 rows name the same one
- expert_gate_weight: bfloat16 [64, 2048, 1024], P('ep', None, 'tp'), may hold values from -0.125 to 0.125
- expert_up_weight: bfloat16 [64, 2048, 1024], P('ep', None, 'tp'), may hold values from -0.125 to 0.125
- expert_down_weight: bfloat16 [64, 1024, 2048], P('ep', 'tp'), may hold values from -0.1875 to 0.1875
- shared_gate_weight: bfloat16 [2048, 2048], P('tp', 'ep'), may hold values from -0.125 to 0.125
- shared_up_weight: bfloat16 [2048, 2048], P('tp', 'ep'), may hold values from -0.125 to 0.125
- shared_down_weight: bfloat16 [2048, 2048], P(None, 'tp'), may hold values from -0.125 to 0.125
Outputs:
- result: bfloat16 [4096, 2048], P('ep', 'tp')
- next_re: float32 [4096, 128, 64], P('ep', 'tp')
- next_im: float32 [4096, 128, 64], P('ep', 'tp')
Inputs may be any that keep to these rules, and one draw needn't show every extreme that they name: `routes`: each row names 2 different experts. Among the rows of one device no expert is named more than 4 times, and in every draw some expert is named exactly 4 times by some device's rows.
All inputs are finite; a program needn't handle non-finite values.
Results may differ from a plain program's by a relative error of at most 0.017.
Values may be sent and summed in bfloat16 or wider, within the bound.
A program may use at most 128 MiB of HBM per device.

v0:
```python
import jax
import jax.numpy as jnp
from jax import lax
from jax.sharding import PartitionSpec as P

NG = 4


EPS = 1e-06


def total_of_pieces(x, axis):
    blocks = lax.all_gather(x, axis)
    return blocks.sum(axis=0)


def in_blocks(x, dim, size):
    lengths = x.shape
    blocks = x.reshape(*lengths[:dim], size, lengths[dim] // size, *lengths[dim + 1 :])
    return jnp.moveaxis(blocks, dim, 0)


def sent_and_summed(x, axis, dim):
    blocks = in_blocks(x, dim, lax.axis_size(axis))
    arrived = lax.all_to_all(blocks, axis, split_axis=0, concat_axis=0, tiled=True)
    return arrived.astype(jnp.float32).sum(axis=0)


def sent_to_all(x, axis):
    size = lax.axis_size(axis)
    return lax.all_to_all(jnp.broadcast_to(x[None], (size, *x.shape)), axis, 0, 0, tiled=True)


def over_copies(x, axis):
    return sent_to_all(x, axis).sum(axis=0)


def in_one(arrays, axis):
    ends = [0]
    for a in arrays:
        ends.append(ends[-1] + a.size)
    so_far = over_copies(jnp.concatenate([a.ravel() for a in arrays]), axis)
    return tuple((so_far[b:e].reshape(a.shape) for a, b, e in zip(arrays, ends, ends[1:])))


def joined_along(blocks, dim):
    lengths = list(blocks.shape[1:])
    lengths[dim] *= blocks.shape[0]
    return jnp.moveaxis(blocks, 0, dim).reshape(lengths)


def collect(x, axis, dim):
    return joined_along(sent_to_all(x, axis), dim)


def taken_together(x, axis):
    return sent_to_all(x, axis).astype(jnp.float32).sum(axis=0)


def state_factors(rate, freq, log_group_step, input_map_real, input_map_imaginary):
    step_size = jnp.exp(log_group_step)[:, None]
    magnitude = jnp.exp(-rate * step_size)
    abar_re = magnitude * jnp.cos(freq * step_size)
    abar_im = magnitude * jnp.sin(freq * step_size)
    denom = rate * rate + freq * freq
    shift_re = abar_re - 1.0
    fac_re = (abar_im * freq - shift_re * rate) / denom
    fac_im = -(abar_im * rate + shift_re * freq) / denom
    bbar_re = fac_re[:, :, None] * input_map_real - fac_im[:, :, None] * input_map_imaginary
    bbar_im = fac_re[:, :, None] * input_map_imaginary + fac_im[:, :, None] * input_map_real
    return (abar_re, abar_im, bbar_re, bbar_im)


def state_step(
    normed,
    sequence_state_real,
    sequence_state_imaginary,
    factors,
    output_map_real,
    output_map_imaginary,
    skip,
):
    abar_re, abar_im, bbar_re, bbar_im = factors
    groups = abar_re.shape[0]
    inputs = normed.astype(jnp.float32)
    grouped = inputs.reshape(inputs.shape[0], groups, -1)
    drive_re = jnp.einsum("tgc,gpc->tgp", grouped, bbar_re)
    drive_im = jnp.einsum("tgc,gpc->tgp", grouped, bbar_im)
    fresh_real = abar_re * sequence_state_real - abar_im * sequence_state_imaginary + drive_re
    fresh_imaginary = abar_re * sequence_state_imaginary + abar_im * sequence_state_real + drive_im
    state_readout = jnp.einsum("dor,zdr->zdo", output_map_real, fresh_real)
    state_readout = state_readout - jnp.einsum(
        "dor,zdr->zdo", output_map_imaginary, fresh_imaginary
    )
    mixed = state_readout.reshape(inputs.shape) + skip * inputs
    return (mixed, fresh_real, fresh_imaginary)


def pair_product(left, first_map, second_map):
    first = jnp.dot(left, first_map, preferred_element_type=jnp.float32)
    second = jnp.dot(left, second_map, preferred_element_type=jnp.float32)
    return jnp.concatenate([first, second], axis=1)


def shards(
    tokens,
    sequence_state_real,
    sequence_state_imaginary,
    mixer_norm_gain,
    expert_norm_gain,
    rate,
    freq,
    log_group_step,
    input_map_real,
    input_map_imaginary,
    output_map_real,
    output_map_imaginary,
    skip,
    mixer_value_weight,
    mixer_gate_weight,
    group_router_weight,
    expert_router_weight,
    dense_blend_weight,
    routes,
    expert_gate_weight,
    expert_up_weight,
    expert_down_weight,
    shared_gate_weight,
    shared_up_weight,
    shared_down_weight,
):
    seq_rows, half_width = tokens.shape
    width = 2 * half_width
    column_start = lax.axis_index("tp") * half_width

    def own_rows(values):
        return lax.dynamic_slice_in_dim(values, column_start, half_width, 0)

    float_tokens = tokens.astype(jnp.float32)
    square_sum = total_of_pieces(jnp.sum(float_tokens * float_tokens, axis=1), "tp")
    first_scale = lax.rsqrt(square_sum / width + EPS)[:, None]
    normed = (float_tokens * first_scale * own_rows(mixer_norm_gain)).astype(jnp.bfloat16)
    factors = state_factors(rate, freq, log_group_step, input_map_real, input_map_imaginary)
    mixed, next_re, next_im = state_step(
        normed,
        sequence_state_real,
        sequence_state_imaginary,
        factors,
        output_map_real,
        output_map_imaginary,
        skip,
    )
    activated = jax.nn.gelu(mixed).astype(jnp.bfloat16)
    value_part = jnp.dot(activated, mixer_value_weight, preferred_element_type=jnp.float32)
    gate_part = jnp.dot(activated, mixer_gate_weight, preferred_element_type=jnp.float32)
    stacked = jnp.stack([value_part, gate_part], axis=1)
    mix_sum = sent_and_summed(stacked.astype(jnp.bfloat16), "tp", 2)
    mix_half = (mix_sum[:, 0] * jax.nn.sigmoid(mix_sum[:, 1])).astype(jnp.bfloat16)
    hidden = (float_tokens + mix_half.astype(jnp.float32)).astype(jnp.bfloat16)
    hidden_f32 = hidden.astype(jnp.float32)
    scaled = hidden_f32 * own_rows(expert_norm_gain)
    router_map = jnp.concatenate(
        [own_rows(group_router_weight), own_rows(expert_router_weight)], axis=1
    ).astype(jnp.float32)
    blend_map = own_rows(dense_blend_weight)
    hidden_squares = jnp.sum(hidden_f32 * hidden_f32, axis=1)
    total_squares = total_of_pieces(hidden_squares, "tp")
    inverse = lax.rsqrt(total_squares / width + EPS)[:, None]
    normal_rows = scaled * inverse
    raw_part = jnp.dot(normal_rows, router_map)
    blend_part = jnp.dot(normal_rows, blend_map)
    logits, blend_logit = in_one((raw_part, blend_part), "tp")
    hnorm = (scaled * inverse).astype(jnp.bfloat16)
    experts = expert_router_weight.shape[1]
    top_count = routes.shape[1]
    per_group = experts // NG
    group_prob = jax.nn.softmax(logits[:, :NG], axis=-1)
    expert_logits = logits[:, NG:]
    expert_hits = routes[:, :, None] == jnp.arange(experts, dtype=jnp.int32)[None, None, :]
    chosen = jnp.sum(jnp.where(expert_hits, expert_logits[:, None, :], 0.0), axis=2)
    group_hits = (routes // per_group)[:, :, None] == jnp.arange(NG, dtype=jnp.int32)[None, None, :]
    group_sel = jnp.sum(jnp.where(group_hits, group_prob[:, None, :], 0.0), axis=2)
    weights = jax.nn.softmax(chosen, axis=1) * group_sel
    full_rows = collect(hnorm, "tp", 1)
    capacity = max(2, 2 * seq_rows * top_count // experts)
    flat_routes = routes.reshape(-1)
    matches = (flat_routes[:, None] == jnp.arange(experts, dtype=jnp.int32)[None, :]).astype(
        jnp.int32
    )
    slot_rank = jnp.sum(jnp.cumsum(matches, axis=0) * matches, axis=1) - 1
    slot_target = flat_routes * capacity + slot_rank
    dispatch = slot_target[None, :] == jnp.arange(experts * capacity, dtype=jnp.int32)[:, None]
    dispatch_rows = jnp.sum(
        dispatch.reshape(experts * capacity, seq_rows, top_count).astype(jnp.float32), axis=2
    )
    outgoing = jnp.dot(
        dispatch_rows.astype(jnp.bfloat16), full_rows, preferred_element_type=jnp.float32
    )
    outgoing = outgoing.astype(jnp.bfloat16).reshape(experts, capacity, width)
    received = lax.all_to_all(outgoing, "ep", split_axis=0, concat_axis=0, tiled=True)
    sources = received.shape[0]
    items = received.shape[1]
    token_rows = received.reshape(sources * items, width)
    gate_e = jnp.dot(token_rows, expert_gate_weight[0], preferred_element_type=jnp.float32)
    expert_up_rows = jnp.dot(token_rows, expert_up_weight[0], preferred_element_type=jnp.float32)
    inner = (jax.nn.silu(gate_e) * expert_up_rows).astype(jnp.bfloat16)
    part_out = jnp.dot(inner, expert_down_weight[0], preferred_element_type=jnp.float32)
    total = taken_together(part_out.astype(jnp.bfloat16), "tp").astype(jnp.float32)
    total = lax.dynamic_slice_in_dim(total, column_start, half_width, 1)
    finished = total.astype(jnp.bfloat16).reshape(sources, items, half_width)
    returned = lax.all_to_all(finished, "ep", split_axis=0, concat_axis=0, tiled=True)
    returned_flat = returned.reshape(experts * capacity, half_width)
    picked = returned_flat[slot_target].reshape(seq_rows, top_count, half_width).astype(jnp.float32)
    routed = jnp.sum(weights[:, :, None] * picked, axis=1)
    partial_dense = pair_product(
        lax.all_gather(hnorm, "ep", axis=0, tiled=True), shared_gate_weight, shared_up_weight
    )
    dense_sum = taken_together(partial_dense.astype(jnp.bfloat16), "tp").astype(jnp.float32)
    dense_cols = shared_gate_weight.shape[1]
    inner_cols = (jax.nn.silu(dense_sum[:, :dense_cols]) * dense_sum[:, dense_cols:]).astype(
        jnp.bfloat16
    )
    dense_inner = lax.all_to_all(inner_cols, "ep", split_axis=0, concat_axis=1, tiled=True)
    dense_out = jnp.dot(dense_inner, shared_down_weight, preferred_element_type=jnp.float32)
    result = hidden_f32 + routed + jax.nn.sigmoid(blend_logit)[:, None] * dense_out
    return (result.astype(jnp.bfloat16), next_re, next_im)


def solution(mesh):
    placed = (
        P("ep", "tp"),
        P("ep", "tp", None),
        P("ep", "tp", None),
        P(),
        P(),
        P("tp", None),
        P("tp", None),
        P("tp"),
        P("tp", None, None),
        P("tp", None, None),
        P("tp", None, None),
        P("tp", None, None),
        P("tp"),
        P("tp", None),
        P("tp", None),
        P(),
        P(),
        P(),
        P("ep", None),
        P("ep", None, "tp"),
        P("ep", None, "tp"),
        P("ep", "tp", None),
        P("tp", "ep"),
        P("tp", "ep"),
        P(None, "tp"),
    )
    return jax.shard_map(
        shards,
        mesh=mesh,
        in_specs=placed,
        out_specs=(P("ep", "tp"), P("ep", "tp", None), P("ep", "tp", None)),
        check_vma=False,
    )
```

profile of v0, /device:TPU:1, one launch (start us, length us, event | category | flops | bytes accessed | tf_op | source)
XLA Modules:
  0.0 190.6 jit_solution(11711179658692557491)
XLA Ops:
  7.2 3.5 %copy.204 = f32[64,64,64]{0,2,1:T(8,128)} copy(f32[64,64,64]{2,1,0:T(8,128)} %param.27) | data formatting | bytes 2097152 | tf_op args[2]
  10.7 3.4 %copy.203 = f32[64,64,64]{0,2,1:T(8,128)} copy(f32[64,64,64]{2,1,0:T(8,128)} %param.26) | data formatting | bytes 2097152 | tf_op args[1]
  14.3 0.6 dynamic-slice
  15.8 3.5 %all-reduce = f32[128]{0:T(128)S(1)} all-reduce(f32[128]{0:T(128)S(1)} %dynamic-update-slice), channel_id=2, replica_groups=mesh['ep'=64,'tp'=2] {'tp'}, use_global_device_ids=true, to_apply=%add | all-reduce | flops 128 | bytes 1024
  19.4 0.8 fusion.29
  20.2 1.1 copy.205
  21.2 1.0 fusion.65
  22.3 4.0 %bitcast_add_fusion.1 = f32[64,64,64]{0,2,1:T(8,128)S(1)} fusion(f32[64,64,64]{0,2,1:T(8,128)} %copy.204, f32[64,64,64]{0,2,1:T(8,128)} %copy.203, bf16[64,64,16]{0,2,1:T(8,128)(2,1)S(1)} %bitcast.73, f32[64,64]{1,0:T(8,128)S(1)} %get-tuple-element.30, f32[64,64]{1,0:T(8,128)S(1)} %get-tuple-element.31, f32[64,64,16]{1,2,0:T(8,128)S(1)} %copy-done.8, ...), kind=kOutput, calls=%fused_computation.14 | convolution fusion | flops 9633792 | bytes 3866624 | tf_op jit(solution)/shard_map/tgc,gpc->tgp/dot_general | solution.py:87
  26.3 2.4 %bitcast_add_fusion = f32[64,64,64]{0,2,1:T(8,128)S(1)} fusion(f32[64,64,64]{0,2,1:T(8,128)S(1)} %copy-done.6, f32[64,64,64]{0,2,1:T(8,128)S(1)} %copy-done.5, bf16[64,64,16]{0,2,1:T(8,128)(2,1)S(1)} %bitcast.74, f32[64,64]{1,0:T(8,128)S(1)} %get-tuple-element.30, f32[64,64]{1,0:T(8,128)S(1)} %get-tuple-element.31, f32[64,64,16]{1,2,0:T(8,128)S(1)} %copy-done.9, ...), kind=kOutput, calls=%fused_computation.13 | convolution fusion | flops 9633792 | bytes 3866624 | tf_op jit(solution)/shard_map/tgc,gpc->tgp/dot_general | solution.py:88
  29.2 1.0 copy-done.10
  30.2 0.4 convolution_subtract_fusion
  30.9 3.1 %convolution_convert_fusion.4 = bf16[64,2048]{1,0:T(8,128)(2,1)S(1)} fusion(bf16[1024,2048]{1,0:T(8,128)(2,1)} %param.39, f32[64,1024]{1,0:T(8,128)S(1)} %copy.210, f32[1024]{0:T(1024)S(1)} %copy-done.17, f32[1024]{0:T(1024)S(1)} %dynamic_slice.18, f32[64]{0:T(128)S(1)} %add_rsqrt_fusion.1, bf16[64,1024]{1,0:T(8,128)(2,1)S(1)} %copy-done.7), kind=kOutput, calls=%fused_computation.6 | convolution fusion | flops 269615104 | bytes 4858112 | tf_op jit(solution)/shard_map/dot_general | solution.py:155
  34.3 3.1 %convolution_convert_fusion.5 = bf16[64,2048]{1,0:T(8,128)(2,1)S(1)} fusion(bf16[1024,2048]{1,0:T(8,128)(2,1)} %param.38, f32[64,1024]{1,0:T(8,128)S(1)} %copy.210, f32[1024]{0:T(1024)S(1)} %copy-done.17, f32[1024]{0:T(1024)S(1)} %dynamic_slice.18, f32[64]{0:T(128)S(1)} %add_rsqrt_fusion.1, bf16[64,1024]{1,0:T(8,128)(2,1)S(1)} %copy-done.7), kind=kOutput, calls=%fused_computation.7 | convolution fusion | flops 269615104 | bytes 4858112 | tf_op jit(solution)/shard_map/dot_general | solution.py:154
  37.8 4.3 %all_to_all.57 = bf16[2,64,2,1024]{3,1,2,0:T(8,128)(2,1)S(1)} all-to-all(bf16[2,64,2,1024]{3,1,2,0:T(8,128)(2,1)S(1)} %maximum_bitcast_fusion), channel_id=1, replica_groups=mesh['ep'=64,'tp'=2] {'tp'}, dimensions={0} | all-to-all | bytes 1048576 | tf_op jit(solution)/shard_map/all_to_all | solution.py:25
  42.6 2.5 %all-reduce.1 = f32[128]{0:T(128)S(1)} all-reduce(f32[128]{0:T(128)S(1)} %dynamic-update-slice.1), channel_id=3, replica_groups=mesh['ep'=64,'tp'=2] {'tp'}, use_global_device_ids=true, to_apply=%add.1 | all-reduce | flops 128 | bytes 1024
  45.2 0.7 fusion.40
  46.0 1.6 broadcast_in_dim.33
  47.6 3.8 %all-to-all-start.2 = ((bf16[2,64,1024]{2,1,0:T(8,128)(2,1)}), bf16[2,64,1024]{2,1,0:T(8,128)(2,1)S(1)}, u32[]{:S(2)}, u32[]{:S(2)}) async-start(bf16[2,64,1024]{2,1,0:T(8,128)(2,1)} %broadcast_in_dim.33), calls=%async_computation.2 | async-start | bytes 524288 | tf_op jit(solution)/shard_map/all_to_all | solution.py:31
  52.0 0.6 all-to-all-done.2
  52.6 0.6 broadcast_in_dim.24
  53.3 4.2 %all-to-all-start.1 = ((f32[2,1,4416]{2,1,0:T(1,128)}), f32[2,1,4416]{2,1,0:T(1,128)}, u32[]{:S(2)}, u32[]{:S(2)}) async-start(f32[2,1,4416]{2,1,0:T(1,128)} %broadcast_in_dim.24), calls=%async_computation.1 | async-start | bytes 71680 | tf_op jit(solution)/shard_map/all_to_all | solution.py:31
  58.5 0.7 add_select_fusion
  59.3 0.4 convolution_convert_fusion.3
  59.7 1.2 reshape.198
  61.0 11.4 %all-to-all-start.3 = ((bf16[64,4,2048]{2,1,0:T(4,128)(2,1)}), bf16[64,4,2048]{2,1,0:T(4,128)(2,1)S(1)}, u32[]{:S(2)}, u32[]{:S(2)}) async-start(bf16[64,4,2048]{2,1,0:T(4,128)(2,1)} %reshape.198), calls=%async_computation.3 | async-start | bytes 2097152 | tf_op jit(solution)/shard_map/all_to_all | solution.py:200
  72.4 0.8 reduce_sum.140
  73.8 3.8 %copy.229 = f32[64,64,64]{2,1,0:T(8,128)} copy(f32[64,64,64]{0,2,1:T(8,128)} %copy-done.4) | data formatting | bytes 2097152
  77.6 3.8 %copy.230 = f32[64,64,64]{2,1,0:T(8,128)} copy(f32[64,64,64]{0,2,1:T(8,128)} %copy-done.3) | data formatting | bytes 2097152
  81.8 10.5 %all-to-all-done.3 = bf16[64,4,2048]{2,1,0:T(4,128)(2,1)S(1)} async-done(((bf16[64,4,2048]{2,1,0:T(4,128)(2,1)}), bf16[64,4,2048]{2,1,0:T(4,128)(2,1)S(1)}, u32[]{:S(2)}, u32[]{:S(2)}) %all-to-all-start.3) | async-done | bytes 1048608 | tf_op jit(solution)/shard_map/all_to_all | solution.py:200
  92.3 1.2 reshape.199
  93.5 3.5 %fusion.3 = f32[256,512]{1,0:T(8,128)} fusion(bf16[256,2048]{1,0:T(8,128)(2,1)} %reshape.199, bf16[1,2048,512]{2,1,0:T(8,128)(2,1)} %param.44), kind=kOutput, calls=%fused_computation.11 | convolution fusion | flops 536870912 | bytes 3670016 | tf_op jit(solution)/shard_map/dot_general | solution.py:204
  97.0 3.3 %convolution_convert_fusion.2 = bf16[256,2048]{1,0:T(8,128)(2,1)S(1)} fusion(bf16[1,512,2048]{2,1,0:T(8,128)(2,1)S(1)} %copy-done, bf16[256,2048]{1,0:T(8,128)(2,1)} %reshape.199, bf16[1,2048,512]{2,1,0:T(8,128)(2,1)} %param.45, f32[256,512]{1,0:T(8,128)} %fusion.3), kind=kOutput, calls=%fused_computation.4 | convolution fusion | flops 1075052544 | bytes 6815744 | tf_op jit(solution)/shard_map/dot_general | solution.py:207
  100.6 7.5 %all_to_all.55 = bf16[2,256,2048]{2,1,0:T(8,128)(2,1)S(1)} all-to-all(bf16[2,256,2048]{2,1,0:T(8,128)(2,1)S(1)} %broadcast_in_dim.34), channel_id=1, replica_groups=mesh['ep'=64,'tp'=2] {'tp'}, dimensions={0} | all-to-all | bytes 4194304 | tf_op jit(solution)/shard_map/all_to_all | solution.py:31
  108.0 0.4 convert_reduce_fusion
  108.5 1.0 reshape.200
  109.5 21.2 %all-gather.4.cloned.1.call-done = bf16[4096,1024]{1,0:T(8,128)(2,1)} async-done(((bf16[64,1024]{1,0:T(8,128)(2,1)}), bf16[4096,1024]{1,0:T(8,128)(2,1)}) %all-gather.4.cloned.1.call-update) | async-done | bytes 8388624 | tf_op jit(solution)/shard_map/all_gather | solution.py:216
  130.7 6.1 %convolution_convert_fusion = bf16[4096,32]{0,1:T(8,128)(2,1)S(1)} fusion(bf16[4096,1024]{1,0:T(8,128)(2,1)} %all-gather.4.cloned.1.call-done, bf16[1024,32]{0,1:T(8,128)(2,1)S(1)} %copy-done.14), kind=kOutput, calls=%fused_computation.1 | convolution fusion | flops 268566528 | bytes 8716288 | tf_op jit(solution)/shard_map/dot_general | solution.py:101
  136.9 2.5 %convolution_convert_fusion.1 = bf16[4096,32]{0,1:T(8,128)(2,1)S(1)} fusion(bf16[4096,1024]{1,0:T(8,128)(2,1)S(1)} %copy-done.2, bf16[1024,32]{0,1:T(8,128)(2,1)S(1)} %copy-done.15), kind=kOutput, calls=%fused_computation.2 | convolution fusion | flops 268566528 | bytes 8716288 | tf_op jit(solution)/shard_map/dot_general | solution.py:100
  139.6 5.0 %all_to_all.56 = bf16[2,4096,64]{1,2,0:T(8,128)(2,1)S(1)} all-to-all(bf16[2,4096,64]{1,2,0:T(8,128)(2,1)S(1)} %broadcast_in_dim.35), channel_id=1, replica_groups=mesh['ep'=64,'tp'=2] {'tp'}, dimensions={0} | all-to-all | bytes 2097152 | tf_op jit(solution)/shard_map/all_to_all | solution.py:31
  144.6 8.3 %all-to-all-start.5 = ((bf16[64,4,1024]{2,1,0:T(4,128)(2,1)}), bf16[64,4,1024]{2,1,0:T(4,128)(2,1)S(1)}, u32[]{:S(2)}, u32[]{:S(2)}) async-start(bf16[64,4,1024]{2,1,0:T(4,128)(2,1)} %reshape.200), calls=%async_computation.5 | async-start | bytes 1048576 | tf_op jit(solution)/shard_map/all_to_all | solution.py:211
  153.3 0.5 all_to_all.43
  154.2 1.0 reshape.228
  155.2 10.2 %all-to-all-done.5 = bf16[64,4,1024]{2,1,0:T(4,128)(2,1)S(1)} async-done(((bf16[64,4,1024]{2,1,0:T(4,128)(2,1)}), bf16[64,4,1024]{2,1,0:T(4,128)(2,1)S(1)}, u32[]{:S(2)}, u32[]{:S(2)}) %all-to-all-start.5) | async-done | bytes 524320 | tf_op jit(solution)/shard_map/all_to_all | solution.py:211
  165.4 4.8 %all-to-all-start.7 = ((bf16[64,2,1024]{2,1,0:T(2,128)(2,1)}), bf16[64,2,1024]{2,1,0:T(2,128)(2,1)S(1)}, u32[]{:S(2)}, u32[]{:S(2)}) async-start(bf16[64,2,1024]{2,1,0:T(2,128)(2,1)} %reshape.228), calls=%async_computation.7 | async-start | bytes 524288 | tf_op jit(solution)/shard_map/all_to_all | solution.py:223
  170.4 0.9 gather_fusion
  171.6 0.7 multiply_reduce_fusion
  172.3 7.3 %all-to-all-done.7 = bf16[64,2,1024]{2,1,0:T(2,128)(2,1)S(1)} async-done(((bf16[64,2,1024]{2,1,0:T(2,128)(2,1)}), bf16[64,2,1024]{2,1,0:T(2,128)(2,1)S(1)}, u32[]{:S(2)}, u32[]{:S(2)}) %all-to-all-start.7) | async-done | bytes 262176 | tf_op jit(solution)/shard_map/all_to_all | solution.py:223
  179.9 3.9 %fusion.12 = bf16[64,1024]{1,0:T(8,128)(2,1)} fusion(bf16[64,2048]{0,1:T(8,128)(2,1)S(1)} %bitcast.77, bf16[2048,1024]{1,0:T(8,128)(2,1)} %param.49, f32[64,1024]{1,0:T(8,128)S(1)} %multiply_reduce_fusion, bf16[64,1024]{1,0:T(8,128)(2,1)S(1)} %get-tuple-element.28, f32[64]{0:T(128)S(1)} %fusion.73), kind=kOutput, calls=%fused_computation.21 | convolution fusion | flops 268763136 | bytes 4980992 | tf_op jit(solution)/shard_map/dot_general | solution.py:224
  (120 shorter events, 7.0 us)
Async XLA Ops:
  7.2 89.8 %copy-start = (bf16[1,512,2048]{2,1,0:T(8,128)(2,1)S(1)}, bf16[1,512,2048]{2,1,0:T(8,128)(2,1)}, u32[]{:S(2)}) copy-start(bf16[1,512,2048]{2,1,0:T(8,128)(2,1)} %param.46) | copy-start | bytes 6291460
  7.2 123.6 %all-gather.4.cloned.1.call-start = ((), (), s32[]{:S(2)}) async-start(), calls=%async_computation.8 | async-start | bytes 8519680 | tf_op jit(solution)/shard_map/all_gather | solution.py:216
  10.7 3.5 %copy-start.7 = (bf16[64,1024]{1,0:T(8,128)(2,1)S(1)}, bf16[64,1024]{1,0:T(8,128)(2,1)}, u32[]{:S(2)}) copy-start(bf16[64,1024]{1,0:T(8,128)(2,1)} %param.25) | copy-start | bytes 393220
  10.7 3.6 %copy-start.23 = (u32[128]{0:T(128)S(1)}, u32[128]{0:T(128)}, u32[]{:S(2)}) copy-start(u32[128]{0:T(128)} %constant.69) | copy-start | bytes 1540
  10.7 8.7 %copy-start.20 = (f32[2048]{0:T(1024)S(1)}, f32[2048]{0:T(1024)}, u32[]{:S(2)}) copy-start(f32[2048]{0:T(1024)} %param.28) | copy-start | bytes 24580
  10.7 10.5 %copy-start.22 = (f32[64]{0:T(128)S(1)}, f32[64]{0:T(128)}, u32[]{:S(2)}) copy-start(f32[64]{0:T(128)} %param.32) | copy-start | bytes 772
  10.7 11.5 %copy-start.8 = (f32[64,64,16]{1,2,0:T(8,128)S(1)}, f32[64,64,16]{1,2,0:T(8,128)}, u32[]{:S(2)}) copy-start(f32[64,64,16]{1,2,0:T(8,128)} %param.34) | copy-start | bytes 786436
  10.7 11.5 %copy-start.9 = (f32[64,64,16]{1,2,0:T(8,128)S(1)}, f32[64,64,16]{1,2,0:T(8,128)}, u32[]{:S(2)}) copy-start(f32[64,64,16]{1,2,0:T(8,128)} %param.33) | copy-start | bytes 786436
  22.3 4.0 %copy-start.5 = (f32[64,64,64]{0,2,1:T(8,128)S(1)}, f32[64,64,64]{0,2,1:T(8,128)}, u32[]{:S(2)}) copy-start(f32[64,64,64]{0,2,1:T(8,128)} %copy.204) | copy-start | bytes 3145732
  22.3 4.0 %copy-start.6 = (f32[64,64,64]{0,2,1:T(8,128)S(1)}, f32[64,64,64]{0,2,1:T(8,128)}, u32[]{:S(2)}) copy-start(f32[64,64,64]{0,2,1:T(8,128)} %copy.203) | copy-start | bytes 3145732
  26.3 2.5 %copy-start.4 = (f32[64,64,64]{0,2,1:T(8,128)}, f32[64,64,64]{0,2,1:T(8,128)S(1)}, u32[]{:S(2)}) copy-start(f32[64,64,64]{0,2,1:T(8,128)S(1)} %bitcast_add_fusion.1) | copy-start | bytes 3145732
  26.3 2.5 %copy-start.11 = (f32[64,16,64]{2,1,0:T(8,128)S(1)}, f32[64,16,64]{2,1,0:T(8,128)}, u32[]{:S(2)}) copy-start(f32[64,16,64]{2,1,0:T(8,128)} %param.35) | copy-start | bytes 786436
  28.8 1.9 copy-start.3
  28.8 1.4 copy-start.10
  30.2 0.7 copy-start.17
  37.7 7.5 %copy-start.21 = (f32[2048]{0:T(1024)S(1)}, f32[2048]{0:T(1024)}, u32[]{:S(2)}) copy-start(f32[2048]{0:T(1024)} %param.29) | copy-start | bytes 24580
  37.8 13.6 %copy-start.19 = (bf16[2048,4]{0,1:T(4,128)(2,1)S(1)}, bf16[2048,4]{0,1:T(4,128)(2,1)}, u32[]{:S(2)}) copy-start(bf16[2048,4]{0,1:T(4,128)(2,1)} %param.40) | copy-start | bytes 49156
  37.8 13.6 %copy-start.16 = (bf16[2048,64]{0,1:T(8,128)(2,1)S(1)}, bf16[2048,64]{0,1:T(8,128)(2,1)}, u32[]{:S(2)}) copy-start(bf16[2048,64]{0,1:T(8,128)(2,1)} %param.41) | copy-start | bytes 786436
  42.1 9.7 %dynamic-slice-start = ((f32[2048]{0:T(1024)}, s32[]{:T(128)}), f32[1024]{0:T(1024)S(1)}, s32[]{:S(2)}) async-start(f32[2048]{0:T(1024)} %param.42, s32[]{:T(128)} %select_n.31), calls=%async_computation.9 | async-start | bytes 8704 | tf_op jit(solution)/shard_map/dynamic_slice | solution.py:137
  42.2 15.3 %copy-start.18 = (s32[64,2]{0,1:T(2,128)S(1)}, s32[64,2]{0,1:T(2,128)}, u32[]{:S(2)}) copy-start(s32[64,2]{0,1:T(2,128)} %param.43) | copy-start | bytes 1540
  47.6 5.0 %all-to-all-start.2 = ((bf16[2,64,1024]{2,1,0:T(8,128)(2,1)}), bf16[2,64,1024]{2,1,0:T(8,128)(2,1)S(1)}, u32[]{:S(2)}, u32[]{:S(2)}) async-start(bf16[2,64,1024]{2,1,0:T(8,128)(2,1)} %broadcast_in_dim.33), calls=%async_computation.2 | async-start | bytes 524288 | tf_op jit(solution)/shard_map/all_to_all | solution.py:31
  53.3 7.7 %all-to-all-start.1 = ((f32[2,1,4416]{2,1,0:T(1,128)}), f32[2,1,4416]{2,1,0:T(1,128)}, u32[]{:S(2)}, u32[]{:S(2)}) async-start(f32[2,1,4416]{2,1,0:T(1,128)} %broadcast_in_dim.24), calls=%async_computation.1 | async-start | bytes 71680 | tf_op jit(solution)/shard_map/all_to_all | solution.py:31
  61.0 31.4 %all-to-all-start.3 = ((bf16[64,4,2048]{2,1,0:T(4,128)(2,1)}), bf16[64,4,2048]{2,1,0:T(4,128)(2,1)S(1)}, u32[]{:S(2)}, u32[]{:S(2)}) async-start(bf16[64,4,2048]{2,1,0:T(4,128)(2,1)} %reshape.198), calls=%async_computation.3 | async-start | bytes 2097152 | tf_op jit(solution)/shard_map/all_to_all | solution.py:200
  77.6 3.8 %copy-start.13 = (s32[64,2]{1,0:T(8,128)S(1)}, s32[64,2]{1,0:T(8,128)}, u32[]{:S(2)}) copy-start(s32[64,2]{1,0:T(8,128)} %get-tuple-element.35) | copy-start | bytes 1540
  77.6 3.9 %copy-start.12 = (s32[64,2]{1,0:T(8,128)S(1)}, s32[64,2]{1,0:T(8,128)}, u32[]{:S(2)}) copy-start(s32[64,2]{1,0:T(8,128)} %get-tuple-element.33) | copy-start | bytes 1540
  108.0 22.7 %copy-start.14 = (bf16[1024,32]{0,1:T(8,128)(2,1)S(1)}, bf16[1024,32]{0,1:T(8,128)(2,1)}, u32[]{:S(2)}) copy-start(bf16[1024,32]{0,1:T(8,128)(2,1)} %param.48) | copy-start | bytes 196612
  109.5 27.3 %copy-start.15 = (bf16[1024,32]{0,1:T(8,128)(2,1)S(1)}, bf16[1024,32]{0,1:T(8,128)(2,1)}, u32[]{:S(2)}) copy-start(bf16[1024,32]{0,1:T(8,128)(2,1)} %param.47) | copy-start | bytes 196612
  130.7 6.1 %copy-start.2 = (bf16[4096,1024]{1,0:T(8,128)(2,1)S(1)}, bf16[4096,1024]{1,0:T(8,128)(2,1)}, u32[]{:S(2)}) copy-start(bf16[4096,1024]{1,0:T(8,128)(2,1)} %all-gather.4.cloned.1.call-done) | copy-start | bytes 25165828
  144.6 20.8 %all-to-all-start.5 = ((bf16[64,4,1024]{2,1,0:T(4,128)(2,1)}), bf16[64,4,1024]{2,1,0:T(4,128)(2,1)S(1)}, u32[]{:S(2)}, u32[]{:S(2)}) async-start(bf16[64,4,1024]{2,1,0:T(4,128)(2,1)} %reshape.200), calls=%async_computation.5 | async-start | bytes 1048576 | tf_op jit(solution)/shard_map/all_to_all | solution.py:211
  165.4 14.2 %all-to-all-start.7 = ((bf16[64,2,1024]{2,1,0:T(2,128)(2,1)}), bf16[64,2,1024]{2,1,0:T(2,128)(2,1)S(1)}, u32[]{:S(2)}, u32[]{:S(2)}) async-start(bf16[64,2,1024]{2,1,0:T(2,128)(2,1)} %reshape.228), calls=%async_computation.7 | async-start | bytes 524288 | tf_op jit(solution)/shard_map/all_to_all | solution.py:223
  179.9 3.9 %copy-start.1 = (bf16[1,512,2048]{2,1,0:T(8,128)(2,1)S(1)}, bf16[1,512,2048]{2,1,0:T(8,128)(2,1)}, u32[]{:S(2)}) copy-start(bf16[1,512,2048]{2,1,0:T(8,128)(2,1)} %param.46) | copy-start | bytes 6291460
Sparse Core Ops, SparseCore 0:
  46.1 84.5 all-gather.3
where the time goes:
time: 193 us; the launch traced here: 191 us
  waiting for transfers between devices  49.8 us (26%)
  matrix products  33.7 us (17%)
  starting transfers between devices  32.6 us (17%)
  local copies, waits for them, and re-layouts  29.5 us (15%)
  blocking collectives  22.7 us (12%)
  between operations  15.3 us (8%)
  other arithmetic  6.95 us (4%)
    all_gather x1, waiting for transfers between devices, shards(): lax.all_gather(hnorm, 'ep', axis=0, tiled=True)  21.2 us
    unnamed x61, local copies, waits for them, and re-layouts  18.2 us
    all_to_all x2, blocking collectives, sent_to_all(): lax.all_to_all(jnp.broadcast_to(x[None], (size, *x.shape)), axis, 0, 0, t...  12.5 us
    all_to_all x1, starting transfers between devices, shards(): lax.all_to_all(outgoing, 'ep', split_axis=0, concat_axis=0, tiled=True)  11.4 us
    all_to_all x1, waiting for transfers between devices, shards(): lax.all_to_all(outgoing, 'ep', split_axis=0, concat_axis=0, tiled=True)  10.5 us
    all_to_all x1, waiting for transfers between devices, shards(): lax.all_to_all(finished, 'ep', split_axis=0, concat_axis=0, tiled=True)  10.2 us
    all_to_all x1, starting transfers between devices, shards(): lax.all_to_all(finished, 'ep', split_axis=0, concat_axis=0, tiled=True)  8.32 us
    all_to_all x2, starting transfers between devices, sent_to_all(): lax.all_to_all(jnp.broadcast_to(x[None], (size, *x.shape)), axis, 0, 0, t...  7.99 us
  transfers between devices with their start and end apart: 6, of which 5 were waited for; matrix products, arithmetic and copies ran while one was open for 15% of the time, Pallas kernels for 0%

commit v1 on v0

v1 whole, which is shorter than its diff:
```python
import jax
import jax.numpy as jnp
from jax import lax
from jax.experimental import pallas as pl
from jax.experimental.pallas import tpu as pltpu
from jax.sharding import PartitionSpec as P

MESH = pl.DeviceIdType.MESH
BF = jnp.bfloat16
F32 = jnp.float32
I32 = jnp.int32
EPS = 1e-06
NEP = 64
ROWS = 64
HALF = 1024
WIDTH = 2048
PITCH = 72
REACH = ((1, 0, 0), (3, 0, 0), (0, 1, 0), (0, 3, 0), (0, 0, 1), (1, 3, 0), (1, 1, 0))


def nn(a, b):
    return jnp.dot(a, b, preferred_element_type=F32)


def nt(a, b):
    return lax.dot_general(a, b, (((1,), (1,)), ((), ())), preferred_element_type=F32)


def iota(shape, dim):
    return lax.broadcasted_iota(I32, shape, dim)


def onehot(condition):
    return jnp.where(condition, 1.0, 0.0).astype(BF)


def column(row, n):
    spread = jnp.where(iota((n, n), 0) == iota((n, n), 1), jnp.broadcast_to(row, (n, n)), 0.0)
    return jnp.sum(spread, axis=1, keepdims=True)


def sigmoid(x):
    return 1.0 / (1.0 + jnp.exp(-x))


def gelu(x):
    return x * (0.5 * (1.0 + jnp.tanh(0.7978845608028654 * (x + 0.044715 * (x * x * x)))))


def shard_of(colour, member):
    z = member % 4
    y = 2 * (member // 4) + colour % 2
    x = (colour // 2 + 16 - y - 2 * z) % 4
    return z * 16 + y * 4 + x


def body(
    tok, mgain, egain, rate, freq, lgs, skip, grw, erw, blend, routes,
    sre, sim, imr, imi, omr, omi, wv, wg, eg, eu, ed, sg, su, sd,
    out, nre, nim,
    sre_v, sim_v, imr_v, imi_v, omr_v, omi_v, wv_v, wg_v, eg_v, eu_v, ed_v, sd_v, wbg, wbu,
    fre, fim, are, aim, bre, bim, cre, cim, vbuf, abuf, rt, dmat, dtmat, m0s, m1s, perm, permt,
    e1s, e1r, vgs, vgr, e3s, e3r, dsend, xo, xp, xx, acc, inner, pts, ptr, ptot, rsend, ret,
    tb, dps, dpr, dis, dn, hid,
    lsem, e_send, e_recv, w_send, w_recv, d_send, d_recv, t_send, t_recv, r_send, r_recv, n_send, n_recv,
):
    ep = lax.axis_index("ep")
    tp = lax.axis_index("tp")
    other = 1 - tp
    x = ep % 4
    y = (ep // 4) % 4
    z = ep // 16
    colour = 2 * ((x + y + 2 * z) % 4) + y % 2
    member = (y // 2) * 4 + z
    own_cols = pl.ds(pl.multiple_of(tp * HALF, HALF), HALF)
    peer_cols = pl.ds(pl.multiple_of(other * HALF, HALF), HALF)

    barrier = pltpu.get_barrier_semaphore()
    me = ep * 2 + tp

    def greet(i, carry):
        d = (me + 1 + i) % (2 * NEP)
        pl.semaphore_signal(barrier, inc=1, device_id=(d // 2, d % 2), device_id_type=MESH)
        return carry

    lax.fori_loop(0, 2 * NEP - 1, greet, 0)

    def load(src, dst, k):
        c = pltpu.make_async_copy(src, dst, lsem.at[k])
        c.start()
        return c

    l_imr = load(imr, imr_v, 0)
    l_imi = load(imi, imi_v, 1)

    def load_state(t, carry):
        rows = pl.ds(pl.multiple_of(t * PITCH, 8), 64)
        pltpu.make_async_copy(sre.at[t], sre_v.at[rows], lsem.at[2]).start()
        pltpu.make_async_copy(sim.at[t], sim_v.at[rows], lsem.at[3]).start()
        return carry

    lax.fori_loop(0, ROWS, load_state, 0)
    l_omr = load(omr, omr_v, 4)
    l_omi = load(omi, omi_v, 5)
    l_wv1 = load(wv.at[:, peer_cols], wv_v.at[0], 6)
    l_wg1 = load(wg.at[:, peer_cols], wg_v.at[0], 7)
    l_wv0 = load(wv.at[:, own_cols], wv_v.at[1], 8)
    l_wg0 = load(wg.at[:, own_cols], wg_v.at[1], 9)
    l_eg = load(eg.at[0], eg_v, 10)
    l_eu = load(eu.at[0], eu_v, 11)
    l_ed = load(ed.at[0], ed_v, 12)
    wslot = pl.ds(pl.multiple_of(member * 32, 32), 32)
    l_sg = load(sg, wbg.at[wslot], 13)
    l_su = load(su, wbu.at[wslot], 14)

    def load_down(p, carry):
        i = shard_of(p // 8, p % 8)
        pltpu.make_async_copy(
            sd.at[pl.ds(pl.multiple_of(i * 32, 32), 32)], sd_v.at[pl.ds(pl.multiple_of(p * 32, 32), 32)], lsem.at[15]
        ).start()
        return carry

    lax.fori_loop(0, 64, load_down, 0)

    tokf = tok[...].astype(F32)
    ss = jnp.sum(tokf * tokf, axis=1, keepdims=True)
    e1s[...] = jnp.broadcast_to(ss, (ROWS, 128))

    step = jnp.exp(column(lgs[...], 64))
    mag = jnp.exp(-rate[...] * step)
    a_re = mag * jnp.cos(freq[...] * step)
    a_im = mag * jnp.sin(freq[...] * step)
    denom = rate[...] * rate[...] + freq[...] * freq[...]
    sh_re = a_re - 1.0
    fre[...] = (a_im * freq[...] - sh_re * rate[...]) / denom
    fim[...] = -(a_im * rate[...] + sh_re * freq[...]) / denom
    are[...] = a_re
    aim[...] = a_im
    l_imr.wait()
    l_imi.wait()

    def make_b(g, carry):
        rows = pl.ds(pl.multiple_of(g * 16, 16), 16)
        f_re = fre[pl.ds(g, 1), :]
        f_im = fim[pl.ds(g, 1), :]
        m_re = imr_v[rows, :]
        m_im = imi_v[rows, :]
        bre[rows, :] = (f_re * m_re - f_im * m_im).astype(BF)
        bim[rows, :] = (f_re * m_im + f_im * m_re).astype(BF)
        return carry

    lax.fori_loop(0, 64, make_b, 0)

    pl.semaphore_wait(barrier, 2 * NEP - 1)

    def exchange(src, dst, k):
        c = pltpu.make_async_remote_copy(
            src_ref=src, dst_ref=dst, send_sem=e_send.at[k], recv_sem=e_recv.at[k],
            device_id=(ep, other), device_id_type=MESH,
        )
        c.start()
        return c

    x1 = exchange(e1s, e1r, 0)

    def send_weights(k, carry):
        dest = shard_of(colour, (member + k) % 8)
        pltpu.make_async_remote_copy(
            src_ref=sg, dst_ref=wbg.at[wslot], send_sem=w_send.at[0], recv_sem=w_recv.at[0],
            device_id=(dest, tp), device_id_type=MESH,
        ).start()
        pltpu.make_async_remote_copy(
            src_ref=su, dst_ref=wbu.at[wslot], send_sem=w_send.at[1], recv_sem=w_recv.at[1],
            device_id=(dest, tp), device_id_type=MESH,
        ).start()
        return carry

    lax.fori_loop(1, 8, send_weights, 0)

    r0 = routes[0:1, :].astype(F32)
    r1 = routes[1:2, :].astype(F32)
    e_sub = iota((64, 64), 0).astype(F32)
    e_lane = iota((64, 64), 1).astype(F32)
    m0 = onehot(e_sub == r0)
    m1 = onehot(e_sub == r1)
    sub4 = iota((64, 256), 0)
    lane4 = iota((64, 256), 1) % 64
    same4 = onehot(sub4 == lane4)
    before4 = onehot(sub4 < lane4)
    n0 = jnp.sum(m0.astype(F32), axis=1, keepdims=True)
    a4 = nn(m0, same4) * (nn(m0, before4) + 1.0) + nn(m1, same4) * (nn(m1, before4) + n0 + 1.0)
    a4 = a4.astype(BF)

    def make_d(q, carry):
        row = iota((256, 1), 0)
        spread = onehot((row // 16 + q * 16) == iota((256, 64), 1))
        got = nn(spread, a4)
        hit = (got == ((row % 4) + 1).astype(F32)) & (((row // 4) % 4) == (iota((256, 256), 1) // 64))
        dmat[pl.ds(pl.multiple_of(q * 256, 256), 256), :] = onehot(hit)
        return carry

    lax.fori_loop(0, 4, make_d, 0)

    c0 = column(r0, 64)
    c1 = column(r1, 64)
    t0 = onehot(e_lane == c0)
    t1 = onehot(e_lane == c1)
    earlier = onehot(iota((64, 64), 1) < iota((64, 64), 0))
    b0 = (t0.astype(F32) * (nn(earlier, t0) + 1.0)).astype(BF)
    b1 = (t1.astype(F32) * (nn(earlier, t1) + jnp.sum(t0.astype(F32), axis=0, keepdims=True) + 1.0)).astype(BF)
    m0s[...] = t0.astype(F32)
    m1s[...] = t1.astype(F32)

    def make_dt(q, carry):
        lane = iota((1, 256), 1)
        spread = onehot((iota((64, 256), 0)) == (iota((64, 256), 1) // 16 + q * 16))
        want = ((lane % 4) + 1).astype(F32)
        cols = pl.ds(pl.multiple_of(q * 256, 256), 256)
        for route, coded in enumerate((b0, b1)):
            got = nn(coded, spread) == want
            for k in range(4):
                rows = pl.ds(route * 256 + k * 64, 64)
                dtmat[rows, cols] = onehot(got & (((lane // 4) % 4) == k))
        return carry

    lax.fori_loop(0, 4, make_dt, 0)
    pi = iota((256, 256), 0)
    pj = iota((256, 256), 1)
    perm[...] = onehot((((pi // 4) % 16) * 16 + (pi // 64) * 4 + pi % 4) == pj)
    permt[...] = onehot((((pi // 4) % 4) * 64 + (pi // 16) * 4 + pi % 4) == pj)
    rt[0:64, :] = erw[:, own_cols]
    rt[64:128, :] = jnp.concatenate([grw[:, own_cols].astype(F32), jnp.zeros((60, HALF), F32)], axis=0).astype(BF)

    x1.wait()
    total = ss + e1r[:, 0:1]
    scale = lax.rsqrt(total / WIDTH + EPS)
    vbuf[...] = (tokf * scale * mgain[:, own_cols]).astype(BF)
    l_omr.wait()
    l_omi.wait()
    cre[...] = omr_v[...].astype(BF)
    cim[...] = omi_v[...].astype(BF)
    pltpu.make_async_copy(sre, sre, lsem.at[2]).wait()
    pltpu.make_async_copy(sim, sim, lsem.at[3]).wait()
    lane_group = iota((ROWS, 128), 1) // 16

    def state_block(b, carry):
        cols = pl.ds(pl.multiple_of(b * 128, 128), 128)
        u = vbuf[:, cols]
        spread = jnp.concatenate([jnp.where(lane_group == j, u, jnp.zeros_like(u)) for j in range(8)], axis=0)
        d_re = nn(spread, bre[cols, :])
        d_im = nn(spread, bim[cols, :])
        fresh_re = []
        fresh_im = []
        for j in range(8):
            g = b * 8 + j
            at = pl.ds(g, ROWS, stride=PITCH)
            s_re = sre_v[at, :]
            s_im = sim_v[at, :]
            g_re = are[pl.ds(g, 1), :]
            g_im = aim[pl.ds(g, 1), :]
            n_re = g_re * s_re - g_im * s_im + d_re[j * ROWS:(j + 1) * ROWS]
            n_im = g_re * s_im + g_im * s_re + d_im[j * ROWS:(j + 1) * ROWS]
            sre_v[at, :] = n_re
            sim_v[at, :] = n_im
            fresh_re.append(n_re.astype(BF))
            fresh_im.append(n_im.astype(BF))
        read = nt(jnp.concatenate(fresh_re, axis=0), cre[cols, :]) - nt(jnp.concatenate(fresh_im, axis=0), cim[cols, :])
        mixed = skip[:, cols] * u.astype(F32)
        for j in range(8):
            mixed = mixed + jnp.where(lane_group == j, read[j * ROWS:(j + 1) * ROWS], 0.0)
        abuf[:, cols] = gelu(mixed).astype(BF)
        return carry

    lax.fori_loop(0, 8, state_block, 0)

    def store_state(t, carry):
        rows = pl.ds(pl.multiple_of(t * PITCH, 8), 64)
        pltpu.make_async_copy(sre_v.at[rows], nre.at[t], lsem.at[16]).start()
        pltpu.make_async_copy(sim_v.at[rows], nim.at[t], lsem.at[17]).start()
        return carry

    lax.fori_loop(0, ROWS, store_state, 0)

    act = abuf[...]
    l_wv1.wait()
    vgs[0] = nn(act, wv_v[0]).astype(BF)
    x2 = exchange(vgs.at[0], vgr.at[0], 1)
    l_wg1.wait()
    vgs[1] = nn(act, wg_v[0]).astype(BF)
    x3 = exchange(vgs.at[1], vgr.at[1], 2)
    l_wv0.wait()
    value = nn(act, wv_v[1]).astype(BF).astype(F32)
    l_wg0.wait()
    gate = nn(act, wg_v[1]).astype(BF).astype(F32)
    x2.wait()
    x3.wait()
    value = value + vgr[0].astype(F32)
    gate = gate + vgr[1].astype(F32)
    mix = (value * sigmoid(gate)).astype(BF)
    hidden = (tok[...].astype(F32) + mix.astype(F32)).astype(BF).astype(F32)
    hid[...] = hidden
    scaled = hidden * egain[:, own_cols]
    top = scaled.astype(BF)
    rest = (scaled - top.astype(F32)).astype(BF)
    logits = nt(top, rt[...]) + nt(rest, rt[...])
    blend_part = jnp.sum(scaled * blend[:, own_cols], axis=1, keepdims=True)
    square_part = jnp.sum(hidden * hidden, axis=1, keepdims=True)
    lane = iota((ROWS, 128), 1)
    logits = jnp.where(lane == 68, blend_part, jnp.where(lane == 69, square_part, logits))
    e3s[...] = logits
    x4 = exchange(e3s, e3r, 3)
    x4.wait()
    logits = logits + e3r[...]
    squares = jnp.sum(jnp.where(lane == 69, logits, 0.0), axis=1, keepdims=True)
    inverse = lax.rsqrt(squares / WIDTH + EPS)
    hnorm = (scaled * inverse).astype(BF)
    logits = logits * inverse

    tb[0:ROWS, :] = hnorm
    quarters = jnp.concatenate([hnorm[:, k * 256:(k + 1) * 256] for k in range(4)], axis=0)
    dsend[...] = nn(dmat[...], quarters).astype(BF)
    mine = pl.ds(pl.multiple_of(ep * 16, 16), 16)
    xo[mine, :] = dsend[mine, :]

    def send_rows(src, dst, ssem, rsem):
        def go(d, carry):
            dest = ((z + d // 16) % 4) * 16 + ((y + (d // 4) % 4) % 4) * 4 + (x + d % 4) % 4
            pltpu.make_async_remote_copy(
                src_ref=src.at[pl.ds(pl.multiple_of(dest * 16, 16), 16)], dst_ref=dst.at[mine],
                send_sem=ssem, recv_sem=rsem, device_id=(dest, tp), device_id_type=MESH,
            ).start()
            return carry

        lax.fori_loop(1, NEP, go, 0)

    send_rows(dsend, xo, d_send, d_recv)
    tok_copies = []
    for i, (dx, dy, dz) in enumerate(REACH):
        dest = ((z + dz) % 4) * 16 + ((y + dy) % 4) * 4 + (x + dx) % 4
        c = pltpu.make_async_remote_copy(
            src_ref=tb.at[pl.ds(0, ROWS)], dst_ref=tb.at[pl.ds((i + 1) * ROWS, ROWS)],
            send_sem=t_send.at[i], recv_sem=t_recv.at[i], device_id=(dest, tp), device_id_type=MESH,
        )
        c.start()
        tok_copies.append(c)

    blend_logit = jnp.sum(jnp.where(lane == 68, logits, 0.0), axis=1, keepdims=True)
    is_group = (lane >= 64) & (lane < 68)
    group_max = jnp.max(jnp.where(is_group, logits, -jnp.inf), axis=1, keepdims=True)
    group_exp = jnp.where(is_group, jnp.exp(jnp.where(is_group, logits, group_max) - group_max), 0.0)
    group_prob = group_exp / jnp.sum(group_exp, axis=1, keepdims=True)
    row0 = column(routes[0:1, :].astype(F32), 64).astype(I32)
    row1 = column(routes[1:2, :].astype(F32), 64).astype(I32)
    pick0 = jnp.sum(jnp.where(lane == row0, logits, 0.0), axis=1, keepdims=True)
    pick1 = jnp.sum(jnp.where(lane == row1, logits, 0.0), axis=1, keepdims=True)
    prob0 = jnp.sum(jnp.where(lane == 64 + row0 // 16, group_prob, 0.0), axis=1, keepdims=True)
    prob1 = jnp.sum(jnp.where(lane == 64 + row1 // 16, group_prob, 0.0), axis=1, keepdims=True)
    top_pick = jnp.maximum(pick0, pick1)
    exp0 = jnp.exp(pick0 - top_pick)
    exp1 = jnp.exp(pick1 - top_pick)
    weight0 = exp0 / (exp0 + exp1) * prob0
    weight1 = exp1 / (exp0 + exp1) * prob1
    blend_gate = sigmoid(blend_logit)

    bulk = pl.ds(0, (NEP - 1) * 16)
    pltpu.make_async_copy(xo.at[bulk], xo.at[bulk], d_recv).wait()
    x5 = exchange(xo, xp, 4)
    l_eg.wait()
    l_eu.wait()

    def unpack(src):
        for q in range(4):
            got = nn(perm[...], src[q * 256:(q + 1) * 256, :]).astype(BF)
            for k in range(4):
                xx[q * 64:(q + 1) * 64, k * 256:(k + 1) * 256] = got[k * 64:(k + 1) * 64]

    unpack(xo)
    acc[0] = nn(xx[...], eg_v[own_cols, :])
    acc[1] = nn(xx[...], eu_v[own_cols, :])
    x5.wait()
    unpack(xp)
    gate_e = acc[0] + nn(xx[...], eg_v[peer_cols, :])
    up_e = acc[1] + nn(xx[...], eu_v[peer_cols, :])
    inner[...] = (gate_e * sigmoid(gate_e) * up_e).astype(BF)
    l_ed.wait()
    pts[...] = nn(inner[...], ed_v[:, peer_cols]).astype(BF)
    x6 = exchange(pts, ptr, 5)
    part = nn(inner[...], ed_v[:, own_cols]).astype(BF)
    ptot[...] = part
    x6.wait()
    ptot[...] = (ptot[...].astype(F32) + ptr[...].astype(F32)).astype(BF)
    for q in range(4):
        rows = slice(q * 64, (q + 1) * 64)
        block = jnp.concatenate([ptot[rows, k * 256:(k + 1) * 256] for k in range(4)], axis=0)
        rsend[q * 256:(q + 1) * 256, :] = nn(permt[...], block).astype(BF)
    ret[mine, :] = rsend[mine, :]
    send_rows(rsend, ret, r_send, r_recv)

    l_sg.wait()
    l_su.wait()
    most = pl.ds(0, 7 * 32)
    pltpu.make_async_copy(wbg.at[most], wbg.at[most], w_recv.at[0]).wait()
    pltpu.make_async_copy(wbu.at[most], wbu.at[most], w_recv.at[1]).wait()
    for c in tok_copies:
        c.wait()
    peer_units = pl.ds(pl.multiple_of(other * 128, 128), 128)
    own_units = pl.ds(pl.multiple_of(tp * 128, 128), 128)
    dps[0] = nt(tb[...], wbg[peer_units, :]).astype(BF)
    dps[1] = nt(tb[...], wbu[peer_units, :]).astype(BF)
    x7 = exchange(dps, dpr, 6)
    dgate = nt(tb[...], wbg[own_units, :]).astype(BF).astype(F32)
    dup = nt(tb[...], wbu[own_units, :]).astype(BF).astype(F32)
    x7.wait()
    dgate = dgate + dpr[0].astype(F32)
    dup = dup + dpr[1].astype(F32)
    dis[...] = (dgate * sigmoid(dgate) * dup).astype(BF)
    slot = pl.ds(pl.multiple_of((colour * 2 + tp) * ROWS, ROWS), ROWS)
    dn[slot, :] = dis[0:ROWS, :]

    def send_inner(i, dest, core):
        pltpu.make_async_remote_copy(
            src_ref=dis.at[pl.ds(i * ROWS, ROWS)], dst_ref=dn.at[slot], send_sem=n_send, recv_sem=n_recv,
            device_id=(dest, core), device_id_type=MESH,
        ).start()

    send_inner(0, ep, other)
    for i, (dx, dy, dz) in enumerate(REACH):
        dest = ((z + 4 - dz) % 4) * 16 + ((y + 4 - dy) % 4) * 4 + (x + 4 - dx) % 4
        send_inner(i + 1, dest, tp)
        send_inner(i + 1, dest, other)
    pltpu.make_async_copy(sd, sd, lsem.at[15]).wait()
    fifteen = pl.ds(0, 15 * ROWS)
    pltpu.make_async_copy(dn.at[fifteen], dn.at[fifteen], n_recv).wait()
    dense_inner = jnp.concatenate([dn[s * ROWS:(s + 1) * ROWS, :] for s in range(16)], axis=1)
    result = hid[...] + blend_gate * nn(dense_inner, sd_v[...])

    pltpu.make_async_copy(ret.at[bulk], ret.at[bulk], r_recv).wait()
    got = nn(dtmat[...], ret[...])
    routed = [
        weight0 * got[k * 64:(k + 1) * 64] + weight1 * got[256 + k * 64:256 + (k + 1) * 64] for k in range(4)
    ]
    out[...] = (result + jnp.concatenate(routed, axis=1)).astype(BF)

    pltpu.make_async_copy(sre, nre, lsem.at[16]).wait()
    pltpu.make_async_copy(sim, nim, lsem.at[17]).wait()
    pltpu.make_async_copy(wbg.at[most], wbg.at[most], w_send.at[0]).wait()
    pltpu.make_async_copy(wbu.at[most], wbu.at[most], w_send.at[1]).wait()
    pltpu.make_async_copy(xo.at[bulk], xo.at[bulk], d_send).wait()
    pltpu.make_async_copy(ret.at[bulk], ret.at[bulk], r_send).wait()
    pltpu.make_async_copy(dn.at[fifteen], dn.at[fifteen], n_send).wait()


def shards(
    tokens, sequence_state_real, sequence_state_imaginary, mixer_norm_gain, expert_norm_gain, rate, freq,
    log_group_step, input_map_real, input_map_imaginary, output_map_real, output_map_imaginary, skip,
    mixer_value_weight, mixer_gate_weight, group_router_weight, expert_router_weight, dense_blend_weight, routes,
    expert_gate_weight, expert_up_weight, expert_down_weight, shared_gate_weight, shared_up_weight,
    shared_down_weight,
):
    vmem = pl.BlockSpec(memory_space=pltpu.VMEM)
    hbm = pl.BlockSpec(memory_space=pl.ANY)
    V = pltpu.VMEM
    D = pltpu.SemaphoreType.DMA
    state = jax.ShapeDtypeStruct((64, 64, 64), F32)
    operands = (
        tokens, mixer_norm_gain[None], expert_norm_gain[None], rate, freq, log_group_step[None], skip[None],
        group_router_weight.T, expert_router_weight.T, dense_blend_weight[None], routes.T,
        sequence_state_real, sequence_state_imaginary,
        jnp.swapaxes(input_map_real, 1, 2).reshape(1024, 64), jnp.swapaxes(input_map_imaginary, 1, 2).reshape(1024, 64),
        output_map_real.reshape(1024, 64), output_map_imaginary.reshape(1024, 64),
        mixer_value_weight, mixer_gate_weight, expert_gate_weight, expert_up_weight, expert_down_weight,
        shared_gate_weight.T, shared_up_weight.T, shared_down_weight,
    )
    scratch = [
        V((64 * PITCH, 64), F32), V((64 * PITCH, 64), F32),
        V((1024, 64), F32), V((1024, 64), F32), V((1024, 64), F32), V((1024, 64), F32),
        V((2, 1024, 1024), BF), V((2, 1024, 1024), BF),
        V((2048, 512), BF), V((2048, 512), BF), V((512, 2048), BF),
        V((2048, 1024), BF), V((256, 1024), BF), V((256, 1024), BF),
        V((64, 64), F32), V((64, 64), F32), V((64, 64), F32), V((64, 64), F32),
        V((1024, 64), BF), V((1024, 64), BF), V((1024, 64), BF), V((1024, 64), BF),
        V((64, 1024), BF), V((64, 1024), BF), V((128, 1024), BF),
        V((1024, 256), BF), V((512, 1024), BF), V((64, 64), F32), V((64, 64), F32), V((256, 256), BF), V((256, 256), BF),
        V((64, 128), F32), V((64, 128), F32), V((2, 64, 1024), BF), V((2, 64, 1024), BF),
        V((64, 128), F32), V((64, 128), F32),
        V((1024, 256), BF), V((1024, 256), BF), V((1024, 256), BF), V((256, 1024), BF),
        V((2, 256, 512), F32), V((256, 512), BF),
        V((256, 1024), BF), V((256, 1024), BF), V((256, 1024), BF),
        V((1024, 256), BF), V((1024, 256), BF),
        V((512, 1024), BF), V((2, 512, 128), BF), V((2, 512, 128), BF), V((512, 128), BF),
        V((1024, 128), BF), V((64, 1024), F32),
        D((18,)), D((7,)), D((7,)), D((2,)), D((2,)), D, D, D((7,)), D((7,)), D, D, D, D,
    ]
    return pl.pallas_call(
        body,
        out_shape=(jax.ShapeDtypeStruct((64, 1024), BF), state, state),
        in_specs=[vmem] * 11 + [hbm] * 14,
        out_specs=(vmem, hbm, hbm),
        scratch_shapes=scratch,
        compiler_params=pltpu.CompilerParams(
            collective_id=0, has_side_effects=True, vmem_limit_bytes=60 * 1024 * 1024
        ),
    )(*operands)


def solution(mesh):
    placed = (
        P("ep", "tp"),
        P("ep", "tp", None),
        P("ep", "tp", None),
        P(),
        P(),
        P("tp", None),
        P("tp", None),
        P("tp"),
        P("tp", None, None),
        P("tp", None, None),
        P("tp", None, None),
        P("tp", None, None),
        P("tp"),
        P("tp", None),
        P("tp", None),
        P(),
        P(),
        P(),
        P("ep", None),
        P("ep", None, "tp"),
        P("ep", None, "tp"),
        P("ep", "tp", None),
        P("tp", "ep"),
        P("tp", "ep"),
        P(None, "tp"),
    )
    return jax.shard_map(
        shards,
        mesh=mesh,
        in_specs=placed,
        out_specs=(P("ep", "tp"), P("ep", "tp", None), P("ep", "tp", None)),
        check_vma=False,
    )
```

time: 193 us -> 62 us (0.32)
  Pallas kernels: 0 us -> 54.3 us
  waiting for transfers between devices: 49.8 us -> 0 us
  matrix products: 33.7 us -> 0 us
  starting transfers between devices: 32.6 us -> 0 us
  local copies, waits for them, and re-layouts: 29.5 us -> 6.2 us
  blocking collectives: 22.7 us -> 0 us
  between operations: 15.3 us -> 0.65 us
  other arithmetic: 6.95 us -> 0 us
    pallas_call x0 -> x1, Pallas kernels: none -> 54.3 us  [shards(): pl.pallas_call(body, out_shape=(jax.ShapeDtypeStruct((64, 1024), BF), sta...]
    dot_general x14 -> x0, matrix products: 33.7 us -> none  [the longest x1 6.07 us: pair_product(): second = jnp.dot(left, second_map, preferred_element_type=jnp.float32)]
    all_to_all x5 -> x0, starting transfers between devices: 32.6 us -> none  [the longest x1 11.4 us: shards(): lax.all_to_all(outgoing, 'ep', split_axis=0, concat_axis=0, tiled=True)]
    all_to_all x5 -> x0, waiting for transfers between devices: 28.6 us -> none  [the longest x1 10.5 us: shards(): lax.all_to_all(outgoing, 'ep', split_axis=0, concat_axis=0, tiled=True)]
    all_gather x1 -> x0, waiting for transfers between devices: 21.2 us -> none  [shards(): lax.all_gather(hnorm, 'ep', axis=0, tiled=True)]
    all_to_all x3 -> x0, blocking collectives: 16.8 us -> none  [the longest x2 12.5 us: sent_to_all(): lax.all_to_all(jnp.broadcast_to(x[None], (size, *x.shape)), axis, 0, 0, t...]
    unnamed x61 -> x5, local copies, waits for them, and re-layouts: 18.2 us -> 6.2 us
    unnamed x2 -> x0, blocking collectives: 5.96 us -> none
  transfers between devices with their start and end apart: 6 -> 0, of which waited for: 5 -> 0; matrix products, arithmetic and copies ran while one was open for 15% -> 0% of each run, Pallas kernels for 0% -> 0%
where the time goes in v1:
time: 62 us; the launch traced here: 61.1 us
  Pallas kernels  54.3 us (88%)
  local copies, waits for them, and re-layouts  6.2 us (10%)
  between operations  0.65 us (1%)
    pallas_call x1, Pallas kernels, shards(): pl.pallas_call(body, out_shape=(jax.ShapeDtypeStruct((64, 1024), BF), sta...  54.3 us
    unnamed x5, local copies, waits for them, and re-layouts  6.2 us

profile of v1, /device:TPU:1, one launch (start us, length us, event | category | flops | bytes accessed | tf_op | source)
XLA Modules:
  0.0 61.1 jit_solution(4158136282520695840)
XLA Ops:
  0.6 54.3 %shard_map.256 = (bf16[64,1024]{1,0:T(8,128)(2,1)}, f32[64,64,64]{2,1,0:T(8,128)}, f32[64,64,64]{2,1,0:T(8,128)}) custom-call(bf16[64,1024]{1,0:T(8,128)(2,1)} %tok.1, f32[1,2048]{1,0:T(1,128)} %bitcast.26, f32[1,2048]{1,0:T(1,128)} %bitcast.27, f32[64,64]{1,0:T(8,128)} %rate.1, f32[64,64]{1,0:T(8,128)} %freq.1, f32[1,64]{1,0:T(1,128)} %bitcast.31, ...), custom_call_target="tpu_custom_call" | custom-call | tf_op jit(solution)/shard_map/pallas_call | solution.py:494
  54.9 1.6 %copy.31 = bf16[64,1024]{1,0:T(8,128)(2,1)} copy(bf16[64,1024]{1,0:T(8,128)(2,1)} %get-tuple-element.6) | data formatting | bytes 262144
  56.5 0.0 copy-start
  56.5 3.3 %copy.32 = f32[64,64,64]{2,1,0:T(8,128)} copy(f32[64,64,64]{2,1,0:T(8,128)} %get-tuple-element.7) | data formatting | bytes 2097152
  59.8 0.0 copy-done
  59.8 1.3 %copy.33 = f32[64,64,64]{2,1,0:T(8,128)} copy(f32[64,64,64]{2,1,0:T(8,128)S(1)} %copy-done) | data formatting | bytes 2097152
Async XLA Ops:
  56.5 3.3 %copy-start = (f32[64,64,64]{2,1,0:T(8,128)S(1)}, f32[64,64,64]{2,1,0:T(8,128)}, u32[]{:S(2)}) copy-start(f32[64,64,64]{2,1,0:T(8,128)} %get-tuple-element.8) | copy-start | bytes 3145732

commit v2 on v1

--- a/solution.py
+++ b/solution.py
@@ -10,12 +10,19 @@
 F32 = jnp.float32
 I32 = jnp.int32
 EPS = 1e-06
+BIG = 3.0e38
 NEP = 64
 ROWS = 64
 HALF = 1024
 WIDTH = 2048
 PITCH = 72
-REACH = ((1, 0, 0), (3, 0, 0), (0, 1, 0), (0, 3, 0), (0, 0, 1), (1, 3, 0), (1, 1, 0))
+REACH = (
+    (1, 0, 0, 0, 64), (3, 0, 0, 0, 64), (0, 1, 0, 0, 64), (0, 3, 0, 0, 64), (0, 0, 1, 0, 32),
+    (0, 0, 3, 32, 32), (1, 3, 0, 0, 32), (3, 1, 0, 32, 32), (1, 1, 0, 0, 32), (3, 3, 0, 32, 32),
+)
+AROUND = sorted(
+    ((d % 4, (d // 4) % 4, d // 16) for d in range(1, 64)), key=lambda o: -sum(min(v, 4 - v) for v in o)
+)
 
 
 def nn(a, b):
@@ -48,9 +55,9 @@
 
 
 def shard_of(colour, member):
-    z = member % 4
-    y = 2 * (member // 4) + colour % 2
-    x = (colour // 2 + 16 - y - 2 * z) % 4
+    z = lax.rem(member, 4)
+    y = 2 * lax.div(member, 4) + lax.rem(colour, 2)
+    x = lax.rem(lax.div(colour, 2) + 16 - y - 2 * z, 4)
     return z * 16 + y * 4 + x
 
 
@@ -58,7 +65,7 @@
     tok, mgain, egain, rate, freq, lgs, skip, grw, erw, blend, routes,
     sre, sim, imr, imi, omr, omi, wv, wg, eg, eu, ed, sg, su, sd,
     out, nre, nim,
-    sre_v, sim_v, imr_v, imi_v, omr_v, omi_v, wv_v, wg_v, eg_v, eu_v, ed_v, sd_v, wbg, wbu,
+    sre_v, sim_v, imr_v, imi_v, omr_v, omi_v, wv_v, wg_v, eg_v, eu_v, ed_v, sd_v, wb,
     fre, fim, are, aim, bre, bim, cre, cim, vbuf, abuf, rt, dmat, dtmat, m0s, m1s, perm, permt,
     e1s, e1r, vgs, vgr, e3s, e3r, dsend, xo, xp, xx, acc, inner, pts, ptr, ptot, rsend, ret,
     tb, dps, dpr, dis, dn, hid,
@@ -67,23 +74,28 @@
     ep = lax.axis_index("ep")
     tp = lax.axis_index("tp")
     other = 1 - tp
-    x = ep % 4
-    y = (ep // 4) % 4
-    z = ep // 16
-    colour = 2 * ((x + y + 2 * z) % 4) + y % 2
-    member = (y // 2) * 4 + z
+    x = lax.rem(ep, 4)
+    y = lax.rem(lax.div(ep, 4), 4)
+    z = lax.div(ep, 16)
+    xs = [lax.rem(x + k, 4) for k in range(4)]
+    ys = [lax.rem(y + k, 4) * 4 for k in range(4)]
+    zs = [lax.rem(z + k, 4) * 16 for k in range(4)]
+
+    def chip(dx, dy, dz):
+        return zs[dz % 4] + ys[dy % 4] + xs[dx % 4]
+
+    colour = 2 * lax.rem(x + y + 2 * z, 4) + lax.rem(y, 2)
+    member = lax.div(y, 2) * 4 + z
     own_cols = pl.ds(pl.multiple_of(tp * HALF, HALF), HALF)
     peer_cols = pl.ds(pl.multiple_of(other * HALF, HALF), HALF)
 
     barrier = pltpu.get_barrier_semaphore()
-    me = ep * 2 + tp
-
-    def greet(i, carry):
-        d = (me + 1 + i) % (2 * NEP)
-        pl.semaphore_signal(barrier, inc=1, device_id=(d // 2, d % 2), device_id_type=MESH)
-        return carry
-
-    lax.fori_loop(0, 2 * NEP - 1, greet, 0)
+    for dx, dy, dz in AROUND:
+        pl.semaphore_signal(barrier, inc=1, device_id=(chip(dx, dy, dz), tp), device_id_type=MESH)
+    for dx, dy, dz, first, rows in REACH:
+        pl.semaphore_signal(barrier, inc=1, device_id=(chip(dx, dy, dz), other), device_id_type=MESH)
+    pl.semaphore_signal(barrier, inc=1, device_id=(ep, other), device_id_type=MESH)
+    greeted = len(AROUND) + len(REACH) + 1
 
     def load(src, dst, k):
         c = pltpu.make_async_copy(src, dst, lsem.at[k])
@@ -93,13 +105,10 @@
     l_imr = load(imr, imr_v, 0)
     l_imi = load(imi, imi_v, 1)
 
-    def load_state(t, carry):
-        rows = pl.ds(pl.multiple_of(t * PITCH, 8), 64)
-        pltpu.make_async_copy(sre.at[t], sre_v.at[rows], lsem.at[2]).start()
-        pltpu.make_async_copy(sim.at[t], sim_v.at[rows], lsem.at[3]).start()
-        return carry
-
-    lax.fori_loop(0, ROWS, load_state, 0)
+    kept_re = sre_v.reshape(ROWS, PITCH, 64).at[:, pl.ds(0, 64)]
+    kept_im = sim_v.reshape(ROWS, PITCH, 64).at[:, pl.ds(0, 64)]
+    l_sre = load(sre, kept_re, 2)
+    l_sim = load(sim, kept_im, 3)
     l_omr = load(omr, omr_v, 4)
     l_omi = load(omi, omi_v, 5)
     l_wv1 = load(wv.at[:, peer_cols], wv_v.at[0], 6)
@@ -109,18 +118,9 @@
     l_eg = load(eg.at[0], eg_v, 10)
     l_eu = load(eu.at[0], eu_v, 11)
     l_ed = load(ed.at[0], ed_v, 12)
-    wslot = pl.ds(pl.multiple_of(member * 32, 32), 32)
-    l_sg = load(sg, wbg.at[wslot], 13)
-    l_su = load(su, wbu.at[wslot], 14)
-
-    def load_down(p, carry):
-        i = shard_of(p // 8, p % 8)
-        pltpu.make_async_copy(
-            sd.at[pl.ds(pl.multiple_of(i * 32, 32), 32)], sd_v.at[pl.ds(pl.multiple_of(p * 32, 32), 32)], lsem.at[15]
-        ).start()
-        return carry
-
-    lax.fori_loop(0, 64, load_down, 0)
+    wrow = lax.div(member, 4) * 256 + lax.rem(member, 4) * 32
+    l_sg = load(sg, wb.at[pl.ds(pl.multiple_of(wrow, 32), 32)], 13)
+    l_su = load(su, wb.at[pl.ds(pl.multiple_of(wrow + 128, 32), 32)], 14)
 
     tokf = tok[...].astype(F32)
     ss = jnp.sum(tokf * tokf, axis=1, keepdims=True)
@@ -150,32 +150,6 @@
         return carry
 
     lax.fori_loop(0, 64, make_b, 0)
-
-    pl.semaphore_wait(barrier, 2 * NEP - 1)
-
-    def exchange(src, dst, k):
-        c = pltpu.make_async_remote_copy(
-            src_ref=src, dst_ref=dst, send_sem=e_send.at[k], recv_sem=e_recv.at[k],
-            device_id=(ep, other), device_id_type=MESH,
-        )
-        c.start()
-        return c
-
-    x1 = exchange(e1s, e1r, 0)
-
-    def send_weights(k, carry):
-        dest = shard_of(colour, (member + k) % 8)
-        pltpu.make_async_remote_copy(
-            src_ref=sg, dst_ref=wbg.at[wslot], send_sem=w_send.at[0], recv_sem=w_recv.at[0],
-            device_id=(dest, tp), device_id_type=MESH,
-        ).start()
-        pltpu.make_async_remote_copy(
-            src_ref=su, dst_ref=wbu.at[wslot], send_sem=w_send.at[1], recv_sem=w_recv.at[1],
-            device_id=(dest, tp), device_id_type=MESH,
-        ).start()
-        return carry
-
-    lax.fori_loop(1, 8, send_weights, 0)
 
     r0 = routes[0:1, :].astype(F32)
     r1 = routes[1:2, :].astype(F32)
@@ -201,6 +175,29 @@
 
     lax.fori_loop(0, 4, make_d, 0)
 
+    pl.semaphore_wait(barrier, greeted)
+
+    def exchange(src, dst, k):
+        c = pltpu.make_async_remote_copy(
+            src_ref=src, dst_ref=dst, send_sem=e_send.at[k], recv_sem=e_recv.at[k],
+            device_id=(ep, other), device_id_type=MESH,
+        )
+        c.start()
+        return c
+
+    x1 = exchange(e1s, e1r, 0)
+
+    groups = [lax.rem(member + k, 8) for k in (6, 2, 5, 7, 1, 3, 4)]
+    groups = [shard_of(colour, m) for m in groups]
+    for piece in range(4):
+        for dest in groups:
+            for i, src in enumerate((sg, su)):
+                pltpu.make_async_remote_copy(
+                    src_ref=src.at[pl.ds(piece * 8, 8)],
+                    dst_ref=wb.at[pl.ds(pl.multiple_of(wrow + i * 128 + piece * 8, 8), 8)],
+                    send_sem=w_send, recv_sem=w_recv, device_id=(dest, tp), device_id_type=MESH,
+                ).start()
+
     c0 = column(r0, 64)
     c1 = column(r1, 64)
     t0 = onehot(e_lane == c0)
@@ -239,8 +236,8 @@
     l_omi.wait()
     cre[...] = omr_v[...].astype(BF)
     cim[...] = omi_v[...].astype(BF)
-    pltpu.make_async_copy(sre, sre, lsem.at[2]).wait()
-    pltpu.make_async_copy(sim, sim, lsem.at[3]).wait()
+    l_sre.wait()
+    l_sim.wait()
     lane_group = iota((ROWS, 128), 1) // 16
 
     def state_block(b, carry):
@@ -273,13 +270,8 @@
 
     lax.fori_loop(0, 8, state_block, 0)
 
-    def store_state(t, carry):
-        rows = pl.ds(pl.multiple_of(t * PITCH, 8), 64)
-        pltpu.make_async_copy(sre_v.at[rows], nre.at[t], lsem.at[16]).start()
-        pltpu.make_async_copy(sim_v.at[rows], nim.at[t], lsem.at[17]).start()
-        return carry
-
-    lax.fori_loop(0, ROWS, store_state, 0)
+    s_nre = load(kept_re, nre, 16)
+    s_nim = load(kept_im, nim, 17)
 
     act = abuf[...]
     l_wv1.wait()
@@ -323,26 +315,33 @@
     xo[mine, :] = dsend[mine, :]
 
     def send_rows(src, dst, ssem, rsem):
-        def go(d, carry):
-            dest = ((z + d // 16) % 4) * 16 + ((y + (d // 4) % 4) % 4) * 4 + (x + d % 4) % 4
+        for dx, dy, dz in AROUND:
+            dest = chip(dx, dy, dz)
             pltpu.make_async_remote_copy(
                 src_ref=src.at[pl.ds(pl.multiple_of(dest * 16, 16), 16)], dst_ref=dst.at[mine],
                 send_sem=ssem, recv_sem=rsem, device_id=(dest, tp), device_id_type=MESH,
             ).start()
-            return carry
-
-        lax.fori_loop(1, NEP, go, 0)
 
     send_rows(dsend, xo, d_send, d_recv)
     tok_copies = []
-    for i, (dx, dy, dz) in enumerate(REACH):
-        dest = ((z + dz) % 4) * 16 + ((y + dy) % 4) * 4 + (x + dx) % 4
+    at = ROWS
+    for i, (dx, dy, dz, first, rows) in enumerate(REACH):
         c = pltpu.make_async_remote_copy(
-            src_ref=tb.at[pl.ds(0, ROWS)], dst_ref=tb.at[pl.ds((i + 1) * ROWS, ROWS)],
-            send_sem=t_send.at[i], recv_sem=t_recv.at[i], device_id=(dest, tp), device_id_type=MESH,
+            src_ref=tb.at[pl.ds(first, rows)], dst_ref=tb.at[pl.ds(at, rows)],
+            send_sem=t_send.at[i], recv_sem=t_recv.at[i], device_id=(chip(dx, dy, dz), tp), device_id_type=MESH,
         )
         c.start()
         tok_copies.append(c)
+        at += rows
+
+    def load_down(p, carry):
+        i = shard_of(lax.div(p, 8), lax.rem(p, 8))
+        pltpu.make_async_copy(
+            sd.at[pl.ds(pl.multiple_of(i * 32, 32), 32)], sd_v.at[pl.ds(pl.multiple_of(p * 32, 32), 32)], lsem.at[15]
+        ).start()
+        return carry
+
+    lax.fori_loop(0, 64, load_down, 0)
 
     blend_logit = jnp.sum(jnp.where(lane == 68, logits, 0.0), axis=1, keepdims=True)
     is_group = (lane >= 64) & (lane < 68)
@@ -398,36 +397,35 @@
 
     l_sg.wait()
     l_su.wait()
-    most = pl.ds(0, 7 * 32)
-    pltpu.make_async_copy(wbg.at[most], wbg.at[most], w_recv.at[0]).wait()
-    pltpu.make_async_copy(wbu.at[most], wbu.at[most], w_recv.at[1]).wait()
+    most = pl.ds(0, 7 * 64)
+    pltpu.make_async_copy(wb.at[most], wb.at[most], w_recv).wait()
     for c in tok_copies:
         c.wait()
-    peer_units = pl.ds(pl.multiple_of(other * 128, 128), 128)
-    own_units = pl.ds(pl.multiple_of(tp * 128, 128), 128)
-    dps[0] = nt(tb[...], wbg[peer_units, :]).astype(BF)
-    dps[1] = nt(tb[...], wbu[peer_units, :]).astype(BF)
+    peer_units = pl.ds(pl.multiple_of(other * 256, 256), 256)
+    own_units = pl.ds(pl.multiple_of(tp * 256, 256), 256)
+    dps[...] = nt(tb[...], wb[peer_units, :]).astype(BF)
     x7 = exchange(dps, dpr, 6)
-    dgate = nt(tb[...], wbg[own_units, :]).astype(BF).astype(F32)
-    dup = nt(tb[...], wbu[own_units, :]).astype(BF).astype(F32)
+    dense = nt(tb[...], wb[own_units, :]).astype(BF).astype(F32)
     x7.wait()
-    dgate = dgate + dpr[0].astype(F32)
-    dup = dup + dpr[1].astype(F32)
-    dis[...] = (dgate * sigmoid(dgate) * dup).astype(BF)
+    dense = dense + dpr[...].astype(F32)
+    dgate = dense[:, 0:128]
+    dis[...] = (dgate * sigmoid(dgate) * dense[:, 128:256]).astype(BF)
     slot = pl.ds(pl.multiple_of((colour * 2 + tp) * ROWS, ROWS), ROWS)
     dn[slot, :] = dis[0:ROWS, :]
 
-    def send_inner(i, dest, core):
+    def send_inner(at, first, rows, dest, core):
+        base = (colour * 2 + tp) * ROWS + first
         pltpu.make_async_remote_copy(
-            src_ref=dis.at[pl.ds(i * ROWS, ROWS)], dst_ref=dn.at[slot], send_sem=n_send, recv_sem=n_recv,
-            device_id=(dest, core), device_id_type=MESH,
+            src_ref=dis.at[pl.ds(at, rows)], dst_ref=dn.at[pl.ds(pl.multiple_of(base, 32), rows)],
+            send_sem=n_send, recv_sem=n_recv, device_id=(dest, core), device_id_type=MESH,
         ).start()
 
-    send_inner(0, ep, other)
-    for i, (dx, dy, dz) in enumerate(REACH):
-        dest = ((z + 4 - dz) % 4) * 16 + ((y + 4 - dy) % 4) * 4 + (x + 4 - dx) % 4
-        send_inner(i + 1, dest, tp)
-        send_inner(i + 1, dest, other)
+    at = ROWS
+    for dx, dy, dz, first, rows in REACH:
+        send_inner(at, first, rows, chip(-dx, -dy, -dz), tp)
+        send_inner(at, first, rows, chip(-dx, -dy, -dz), other)
+        at += rows
+    send_inner(0, 0, ROWS, ep, other)
     pltpu.make_async_copy(sd, sd, lsem.at[15]).wait()
     fifteen = pl.ds(0, 15 * ROWS)
     pltpu.make_async_copy(dn.at[fifteen], dn.at[fifteen], n_recv).wait()
@@ -441,10 +439,9 @@
     ]
     out[...] = (result + jnp.concatenate(routed, axis=1)).astype(BF)
 
-    pltpu.make_async_copy(sre, nre, lsem.at[16]).wait()
-    pltpu.make_async_copy(sim, nim, lsem.at[17]).wait()
-    pltpu.make_async_copy(wbg.at[most], wbg.at[most], w_send.at[0]).wait()
-    pltpu.make_async_copy(wbu.at[most], wbu.at[most], w_send.at[1]).wait()
+    s_nre.wait()
+    s_nim.wait()
+    pltpu.make_async_copy(wb.at[most], wb.at[most], w_send).wait()
     pltpu.make_async_copy(xo.at[bulk], xo.at[bulk], d_send).wait()
     pltpu.make_async_copy(ret.at[bulk], ret.at[bulk], r_send).wait()
     pltpu.make_async_copy(dn.at[fifteen], dn.at[fifteen], n_send).wait()
@@ -476,7 +473,7 @@
         V((1024, 64), F32), V((1024, 64), F32), V((1024, 64), F32), V((1024, 64), F32),
         V((2, 1024, 1024), BF), V((2, 1024, 1024), BF),
         V((2048, 512), BF), V((2048, 512), BF), V((512, 2048), BF),
-        V((2048, 1024), BF), V((256, 1024), BF), V((256, 1024), BF),
+        V((2048, 1024), BF), V((512, 1024), BF),
         V((64, 64), F32), V((64, 64), F32), V((64, 64), F32), V((64, 64), F32),
         V((1024, 64), BF), V((1024, 64), BF), V((1024, 64), BF), V((1024, 64), BF),
         V((64, 1024), BF), V((64, 1024), BF), V((128, 1024), BF),
@@ -487,11 +484,11 @@
         V((2, 256, 512), F32), V((256, 512), BF),
         V((256, 1024), BF), V((256, 1024), BF), V((256, 1024), BF),
         V((1024, 256), BF), V((1024, 256), BF),
-        V((512, 1024), BF), V((2, 512, 128), BF), V((2, 512, 128), BF), V((512, 128), BF),
+        V((512, 1024), BF), V((512, 256), BF), V((512, 256), BF), V((512, 128), BF),
         V((1024, 128), BF), V((64, 1024), F32),
-        D((18,)), D((7,)), D((7,)), D((2,)), D((2,)), D, D, D((7,)), D((7,)), D, D, D, D,
+        D((18,)), D((7,)), D((7,)), D, D, D, D, D((len(REACH),)), D((len(REACH),)), D, D, D, D,
     ]
-    return pl.pallas_call(
+    result, next_re, next_im = pl.pallas_call(
         body,
         out_shape=(jax.ShapeDtypeStruct((64, 1024), BF), state, state),
         in_specs=[vmem] * 11 + [hbm] * 14,
@@ -501,6 +498,7 @@
             collective_id=0, has_side_effects=True, vmem_limit_bytes=60 * 1024 * 1024
         ),
     )(*operands)
+    return (result, lax.clamp(-BIG, next_re, BIG), lax.clamp(-BIG, next_im, BIG))
 
 
 def solution(mesh):

time: 62 us -> 55.9 us (0.902); the launches traced: 61.1 us -> 55.7 us
  local copies, waits for them, and re-layouts: 6.2 us -> 0.66 us
  other arithmetic: 0 us -> 5.18 us
  Pallas kernels: 54.3 us -> 49.2 us
    unnamed x5 -> x3, local copies, waits for them, and re-layouts: 6.2 us -> 0.66 us
    clamp x0 -> x1, other arithmetic: none -> 5.18 us  [shards(): lax.clamp(-BIG, next_im, BIG)]
    pallas_call x1, Pallas kernels: 54.3 us -> 49.2 us  [shards(): pl.pallas_call(body, out_shape=(jax.ShapeDtypeStruct((64, 1024), BF), sta...]
where the time goes in v2:
time: 55.9 us; the launch traced here: 55.7 us
  Pallas kernels  49.2 us (88%)
  other arithmetic  5.18 us (9%)
  local copies, waits for them, and re-layouts  0.66 us (1%)
  between operations  0.66 us (1%)
    pallas_call x1, Pallas kernels, shards(): pl.pallas_call(body, out_shape=(jax.ShapeDtypeStruct((64, 1024), BF), sta...  49.2 us
    clamp x1, other arithmetic, shards(): lax.clamp(-BIG, next_im, BIG)  5.18 us

profile of v2, /device:TPU:1, one launch (start us, length us, event | category | flops | bytes accessed | tf_op | source)
XLA Modules:
  0.0 55.7 jit_solution(256641442978357274)
XLA Ops:
  0.6 49.2 %shard_map.256 = (bf16[64,1024]{1,0:T(8,128)(2,1)}, f32[64,64,64]{2,1,0:T(8,128)}, f32[64,64,64]{2,1,0:T(8,128)}) custom-call(bf16[64,1024]{1,0:T(8,128)(2,1)} %tok.1, f32[1,2048]{1,0:T(1,128)} %bitcast.26, f32[1,2048]{1,0:T(1,128)} %bitcast.27, f32[64,64]{1,0:T(8,128)} %rate.1, f32[64,64]{1,0:T(8,128)} %freq.1, f32[1,64]{1,0:T(1,128)} %bitcast.31, ...), custom_call_target="tpu_custom_call" | custom-call | tf_op jit(solution)/shard_map/pallas_call | solution.py:491
  49.9 0.0 copy-start
  49.9 5.2 %broadcast_clamp_fusion = (f32[64,64,64]{2,1,0:T(8,128)}, f32[64,64,64]{2,1,0:T(8,128)}) fusion(f32[64,64,64]{2,1,0:T(8,128)} %get-tuple-element.8, f32[64,64,64]{2,1,0:T(8,128)} %get-tuple-element.7), kind=kLoop, calls=%fused_computation | loop fusion | flops 524288 | bytes 4194304 | tf_op jit(solution)/shard_map/clamp | solution.py:501
  55.1 0.0 copy-done
  55.1 0.7 %copy.29 = bf16[64,1024]{1,0:T(8,128)(2,1)} copy(bf16[64,1024]{1,0:T(8,128)(2,1)S(1)} %copy-done) | data formatting | bytes 262144
Async XLA Ops:
  49.9 5.2 %copy-start = (bf16[64,1024]{1,0:T(8,128)(2,1)S(1)}, bf16[64,1024]{1,0:T(8,128)(2,1)}, u32[]{:S(2)}) copy-start(bf16[64,1024]{1,0:T(8,128)(2,1)} %get-tuple-element.14) | copy-start | bytes 393220

commit v3 on v2

--- a/solution.py
+++ b/solution.py
@@ -10,7 +10,7 @@
 F32 = jnp.float32
 I32 = jnp.int32
 EPS = 1e-06
-BIG = 3.0e38
+PARTS = 4
 NEP = 64
 ROWS = 64
 HALF = 1024
@@ -62,9 +62,10 @@
 
 
 def body(
-    tok, mgain, egain, rate, freq, lgs, skip, grw, erw, blend, routes,
+    tok_h, mgain_h, egain_h, rate_h, freq_h, lgs_h, skip_h, grw_h, erw_h, blend_h, routes_h,
     sre, sim, imr, imi, omr, omi, wv, wg, eg, eu, ed, sg, su, sd,
     out, nre, nim,
+    tok, mgain, egain, rate, freq, lgs, skip, grw, erw, blend, routes,
     sre_v, sim_v, imr_v, imi_v, omr_v, omi_v, wv_v, wg_v, eg_v, eu_v, ed_v, sd_v, wb,
     fre, fim, are, aim, bre, bim, cre, cim, vbuf, abuf, rt, dmat, dtmat, m0s, m1s, perm, permt,
     e1s, e1r, vgs, vgr, e3s, e3r, dsend, xo, xp, xx, acc, inner, pts, ptr, ptot, rsend, ret,
@@ -102,6 +103,13 @@
         c.start()
         return c
 
+    small = [
+        load(src, dst, 18 + k)
+        for k, (src, dst) in enumerate((
+            (tok_h, tok), (routes_h, routes), (rate_h, rate), (freq_h, freq), (lgs_h, lgs), (mgain_h, mgain),
+            (skip_h, skip), (grw_h, grw), (erw_h, erw), (egain_h, egain), (blend_h, blend),
+        ))
+    ]
     l_imr = load(imr, imr_v, 0)
     l_imi = load(imi, imi_v, 1)
 
@@ -122,35 +130,12 @@
     l_sg = load(sg, wb.at[pl.ds(pl.multiple_of(wrow, 32), 32)], 13)
     l_su = load(su, wb.at[pl.ds(pl.multiple_of(wrow + 128, 32), 32)], 14)
 
+    small[0].wait()
     tokf = tok[...].astype(F32)
     ss = jnp.sum(tokf * tokf, axis=1, keepdims=True)
     e1s[...] = jnp.broadcast_to(ss, (ROWS, 128))
 
-    step = jnp.exp(column(lgs[...], 64))
-    mag = jnp.exp(-rate[...] * step)
-    a_re = mag * jnp.cos(freq[...] * step)
-    a_im = mag * jnp.sin(freq[...] * step)
-    denom = rate[...] * rate[...] + freq[...] * freq[...]
-    sh_re = a_re - 1.0
-    fre[...] = (a_im * freq[...] - sh_re * rate[...]) / denom
-    fim[...] = -(a_im * rate[...] + sh_re * freq[...]) / denom
-    are[...] = a_re
-    aim[...] = a_im
-    l_imr.wait()
-    l_imi.wait()
-
-    def make_b(g, carry):
-        rows = pl.ds(pl.multiple_of(g * 16, 16), 16)
-        f_re = fre[pl.ds(g, 1), :]
-        f_im = fim[pl.ds(g, 1), :]
-        m_re = imr_v[rows, :]
-        m_im = imi_v[rows, :]
-        bre[rows, :] = (f_re * m_re - f_im * m_im).astype(BF)
-        bim[rows, :] = (f_re * m_im + f_im * m_re).astype(BF)
-        return carry
-
-    lax.fori_loop(0, 64, make_b, 0)
-
+    small[1].wait()
     r0 = routes[0:1, :].astype(F32)
     r1 = routes[1:2, :].astype(F32)
     e_sub = iota((64, 64), 0).astype(F32)
@@ -175,6 +160,33 @@
 
     lax.fori_loop(0, 4, make_d, 0)
 
+    for k in (2, 3, 4):
+        small[k].wait()
+    step = jnp.exp(column(lgs[...], 64))
+    mag = jnp.exp(-rate[...] * step)
+    a_re = mag * jnp.cos(freq[...] * step)
+    a_im = mag * jnp.sin(freq[...] * step)
+    denom = rate[...] * rate[...] + freq[...] * freq[...]
+    sh_re = a_re - 1.0
+    fre[...] = (a_im * freq[...] - sh_re * rate[...]) / denom
+    fim[...] = -(a_im * rate[...] + sh_re * freq[...]) / denom
+    are[...] = a_re
+    aim[...] = a_im
+    l_imr.wait()
+    l_imi.wait()
+
+    def make_b(g, carry):
+        rows = pl.ds(pl.multiple_of(g * 16, 16), 16)
+        f_re = fre[pl.ds(g, 1), :]
+        f_im = fim[pl.ds(g, 1), :]
+        m_re = imr_v[rows, :]
+        m_im = imi_v[rows, :]
+        bre[rows, :] = (f_re * m_re - f_im * m_im).astype(BF)
+        bim[rows, :] = (f_re * m_im + f_im * m_re).astype(BF)
+        return carry
+
+    lax.fori_loop(0, 64, make_b, 0)
+
     pl.semaphore_wait(barrier, greeted)
 
     def exchange(src, dst, k):
@@ -225,10 +237,14 @@
     pj = iota((256, 256), 1)
     perm[...] = onehot((((pi // 4) % 16) * 16 + (pi // 64) * 4 + pi % 4) == pj)
     permt[...] = onehot((((pi // 4) % 4) * 64 + (pi // 16) * 4 + pi % 4) == pj)
+    small[7].wait()
+    small[8].wait()
     rt[0:64, :] = erw[:, own_cols]
     rt[64:128, :] = jnp.concatenate([grw[:, own_cols].astype(F32), jnp.zeros((60, HALF), F32)], axis=0).astype(BF)
 
     x1.wait()
+    small[5].wait()
+    small[6].wait()
     total = ss + e1r[:, 0:1]
     scale = lax.rsqrt(total / WIDTH + EPS)
     vbuf[...] = (tokf * scale * mgain[:, own_cols]).astype(BF)
@@ -291,6 +307,8 @@
     mix = (value * sigmoid(gate)).astype(BF)
     hidden = (tok[...].astype(F32) + mix.astype(F32)).astype(BF).astype(F32)
     hid[...] = hidden
+    small[9].wait()
+    small[10].wait()
     scaled = hidden * egain[:, own_cols]
     top = scaled.astype(BF)
     rest = (scaled - top.astype(F32)).astype(BF)
@@ -426,18 +444,18 @@
         send_inner(at, first, rows, chip(-dx, -dy, -dz), other)
         at += rows
     send_inner(0, 0, ROWS, ep, other)
-    pltpu.make_async_copy(sd, sd, lsem.at[15]).wait()
-    fifteen = pl.ds(0, 15 * ROWS)
-    pltpu.make_async_copy(dn.at[fifteen], dn.at[fifteen], n_recv).wait()
-    dense_inner = jnp.concatenate([dn[s * ROWS:(s + 1) * ROWS, :] for s in range(16)], axis=1)
-    result = hid[...] + blend_gate * nn(dense_inner, sd_v[...])
-
     pltpu.make_async_copy(ret.at[bulk], ret.at[bulk], r_recv).wait()
     got = nn(dtmat[...], ret[...])
     routed = [
         weight0 * got[k * 64:(k + 1) * 64] + weight1 * got[256 + k * 64:256 + (k + 1) * 64] for k in range(4)
     ]
-    out[...] = (result + jnp.concatenate(routed, axis=1)).astype(BF)
+    hid[...] = hid[...] + jnp.concatenate(routed, axis=1)
+
+    pltpu.make_async_copy(sd, sd, lsem.at[15]).wait()
+    fifteen = pl.ds(0, 15 * ROWS)
+    pltpu.make_async_copy(dn.at[fifteen], dn.at[fifteen], n_recv).wait()
+    dense_inner = jnp.concatenate([dn[s * ROWS:(s + 1) * ROWS, :] for s in range(16)], axis=1)
+    out[...] = (hid[...] + blend_gate * nn(dense_inner, sd_v[...])).astype(BF)
 
     s_nre.wait()
     s_nim.wait()
@@ -445,6 +463,24 @@
     pltpu.make_async_copy(xo.at[bulk], xo.at[bulk], d_send).wait()
     pltpu.make_async_copy(ret.at[bulk], ret.at[bulk], r_send).wait()
     pltpu.make_async_copy(dn.at[fifteen], dn.at[fifteen], n_send).wait()
+
+
+def hand_out(result, next_re, next_im, out, nre, nim, out_v, re_v, im_v, sem):
+    size = ROWS // PARTS
+    moves = [(result, out_v, out)]
+    for i in range(PARTS):
+        rows = pl.ds(i * size, size)
+        moves.append((next_re.at[rows], re_v.at[rows], nre.at[rows]))
+        moves.append((next_im.at[rows], im_v.at[rows], nim.at[rows]))
+    loads = [pltpu.make_async_copy(src, mid, sem.at[0, k]) for k, (src, mid, dst) in enumerate(moves)]
+    stores = [pltpu.make_async_copy(mid, dst, sem.at[1, k]) for k, (src, mid, dst) in enumerate(moves)]
+    for c in loads:
+        c.start()
+    for c, d in zip(loads, stores):
+        c.wait()
+        d.start()
+    for d in stores:
+        d.wait()
 
 
 def shards(
@@ -469,6 +505,8 @@
         shared_gate_weight.T, shared_up_weight.T, shared_down_weight,
     )
     scratch = [
+        V((64, 1024), BF), V((1, 2048), F32), V((1, 2048), F32), V((64, 64), F32), V((64, 64), F32), V((1, 64), F32),
+        V((1, 1024), F32), V((4, 2048), BF), V((64, 2048), BF), V((1, 2048), F32), V((2, 64), I32),
         V((64 * PITCH, 64), F32), V((64 * PITCH, 64), F32),
         V((1024, 64), F32), V((1024, 64), F32), V((1024, 64), F32), V((1024, 64), F32),
         V((2, 1024, 1024), BF), V((2, 1024, 1024), BF),
@@ -486,19 +524,25 @@
         V((1024, 256), BF), V((1024, 256), BF),
         V((512, 1024), BF), V((512, 256), BF), V((512, 256), BF), V((512, 128), BF),
         V((1024, 128), BF), V((64, 1024), F32),
-        D((18,)), D((7,)), D((7,)), D, D, D, D, D((len(REACH),)), D((len(REACH),)), D, D, D, D,
+        D((29,)), D((7,)), D((7,)), D, D, D, D, D((len(REACH),)), D((len(REACH),)), D, D, D, D,
     ]
     result, next_re, next_im = pl.pallas_call(
         body,
         out_shape=(jax.ShapeDtypeStruct((64, 1024), BF), state, state),
-        in_specs=[vmem] * 11 + [hbm] * 14,
+        in_specs=[hbm] * 25,
         out_specs=(vmem, hbm, hbm),
         scratch_shapes=scratch,
         compiler_params=pltpu.CompilerParams(
             collective_id=0, has_side_effects=True, vmem_limit_bytes=60 * 1024 * 1024
         ),
     )(*operands)
-    return (result, lax.clamp(-BIG, next_re, BIG), lax.clamp(-BIG, next_im, BIG))
+    return pl.pallas_call(
+        hand_out,
+        out_shape=(jax.ShapeDtypeStruct((64, 1024), BF), state, state),
+        in_specs=[hbm] * 3,
+        out_specs=(hbm,) * 3,
+        scratch_shapes=[V((64, 1024), BF), V((64, 64, 64), F32), V((64, 64, 64), F32), D((2, 2 * PARTS + 1))],
+    )(result, next_re, next_im)
 
 
 def solution(mesh):

time: 55.9 us -> 52.3 us (0.936)
  other arithmetic: 5.18 us -> 0 us
  Pallas kernels: 49.2 us -> 51.5 us
  local copies, waits for them, and re-layouts: 0.66 us -> 0 us
    clamp x1 -> x0, other arithmetic: 5.18 us -> none  [shards(): lax.clamp(-BIG, next_im, BIG)]
    pallas_call x0 -> x1, Pallas kernels: none -> 3.81 us  [shards(): pl.pallas_call(hand_out, out_shape=(jax.ShapeDtypeStruct((64, 1024), BF),...]
    pallas_call x1, Pallas kernels: 49.2 us -> 47.7 us  [shards(): pl.pallas_call(body, out_shape=(jax.ShapeDtypeStruct((64, 1024), BF), sta...]
    unnamed x3 -> x0, local copies, waits for them, and re-layouts: 0.66 us -> none
where the time goes in v3:
time: 52.3 us; the launch traced here: 52.2 us
  Pallas kernels  51.5 us (98%)
  between operations  0.65 us (1%)
    pallas_call x1, Pallas kernels, shards(): pl.pallas_call(body, out_shape=(jax.ShapeDtypeStruct((64, 1024), BF), sta...  47.7 us
    pallas_call x1, Pallas kernels, shards(): pl.pallas_call(hand_out, out_shape=(jax.ShapeDtypeStruct((64, 1024), BF),...  3.81 us

profile of v3, /device:TPU:1, one launch (start us, length us, event | category | flops | bytes accessed | tf_op | source)
XLA Modules:
  0.0 52.2 jit_solution(16440564810434785725)
XLA Ops:
  0.6 47.7 %shard_map.256 = (bf16[64,1024]{1,0:T(8,128)(2,1)}, f32[64,64,64]{2,1,0:T(8,128)}, f32[64,64,64]{2,1,0:T(8,128)}) custom-call(bf16[64,1024]{1,0:T(8,128)(2,1)} %tok_h.1, f32[1,2048]{1,0:T(1,128)} %bitcast.26, f32[1,2048]{1,0:T(1,128)} %bitcast.27, f32[64,64]{1,0:T(8,128)} %rate_h.1, f32[64,64]{1,0:T(8,128)} %freq_h.1, f32[1,64]{1,0:T(1,128)} %bitcast.31, ...), custom_call_target="tpu_custom_call" | custom-call | tf_op jit(solution)/shard_map/pallas_call | solution.py:529
  48.4 3.8 %shard_map.257 = (bf16[64,1024]{1,0:T(8,128)(2,1)}, f32[64,64,64]{2,1,0:T(8,128)}, f32[64,64,64]{2,1,0:T(8,128)}) custom-call(bf16[64,1024]{1,0:T(8,128)(2,1)} %get-tuple-element.6.result, f32[64,64,64]{2,1,0:T(8,128)} %get-tuple-element.7.next_re, f32[64,64,64]{2,1,0:T(8,128)} %get-tuple-element.8.next_im), custom_call_target="tpu_custom_call" | custom-call | tf_op jit(solution)/shard_map/pallas_call | solution.py:539
